TPU v7x, 32 devices: a whole 2x2x4 slice. The times are simulated.
32 devices in a mesh: sp: 8 (over z, y), dp: 4 (over x, core).
Axes of the slice: x: 2, y: 2, z: 4, core: 2. Of those that a mesh axis runs over, the one named last changes fastest.
Arguments:
- tokens: bfloat16 [4, 2048, 2048], P('dp', 'sp'), may hold values from -6 to 6
- in_gain: float32 [2048], replicated, may hold values from 0.1 to 1.9
- w_query_down: bfloat16 [2048, 512], P('dp'), may hold values from -0.125 to 0.125
- w_latent_down: bfloat16 [2048, 256], P('dp'), may hold values from -0.125 to 0.125
- w_rope_key: bfloat16 [2048, 64], replicated, may hold values from -0.125 to 0.125
- query_latent_gain: float32 [512], replicated, may hold values from 0.1 to 1.9
- latent_gain: float32 [256], replicated, may hold values from 0.1 to 1.9
- w_query_up: bfloat16 [512, 3072], P('dp', 'sp'), may hold values from -0.25 to 0.25
- w_key_up: bfloat16 [256, 2048], P('dp', 'sp'), may hold values from -0.375 to 0.375
- w_value_up: bfloat16 [256, 2048], P('dp', 'sp'), may hold values from -0.375 to 0.375
- query_gain: float32 [192], replicated, may hold values from 0.5 to 14
- key_gain: float32 [192], replicated, may hold values from 0.5 to 14
- out_gain: float32 [2048], replicated, may hold values from 0.1 to 1.9
- w_out: bfloat16 [2048, 2048], P(('sp', 'dp')), may hold values from -0.125 to 0.125
Outputs:
- result: bfloat16 [4, 2048, 2048], P('dp', 'sp')
All inputs are finite; a program needn't handle non-finite values.
Results may differ from a plain program's by a relative error of at most 0.034.
The roundings to bfloat16 on the way count: a program that leaves them out, or rounds other values in their place, can miss the bound.
Values may be sent and summed in bfloat16 or wider, within the bound.
A program may use at most 64 MiB of HBM per device.

v0:
```python
import functools

import jax
import jax.numpy as jnp
import numpy as np
from jax import lax
from jax.experimental import pallas as pl
from jax.experimental.pallas import tpu as pltpu
from jax.sharding import PartitionSpec as P

HEADS = 16
EPS = 1e-06
THETA = 10000.0
NEG_BIG = -1e30
LOG2E = 1.4426950408889634
NT = (((1,), (1,)), ((), ()))


def rms_scale(values, scaling):
    return values * lax.rsqrt(jnp.mean(values * values, axis=-1, keepdims=True) + EPS) * scaling


def swap_halves(x):
    half = x.shape[-1] // 2
    return jnp.concatenate([x[..., half:], x[..., :half]], axis=-1)


def rotation_table(length, width):
    half = width // 2
    frequency = np.float32(THETA) ** (-np.arange(half, dtype=np.float32) / np.float32(half))
    angles = np.arange(length, dtype=np.float32)[:, None] * frequency[None, :]
    cosine, sine = np.cos(angles), np.sin(angles)
    return np.concatenate([cosine, cosine, -sine, sine], axis=-1).astype(np.float32)


def with_swapped(x):
    return jnp.concatenate([x, swap_halves(x)], axis=-1)


def project_block(i, rows, heads, nope, vd, lq, lkv, rp, wq, wk, wvt, gq, gk, gq2, gk2, table, q_s, k_s, v_s):
    tok = pl.ds(pl.multiple_of(i * rows, rows), rows)
    wide = wq.shape[1] // heads
    rope2 = wide - nope
    inv = 1.0 / (nope + rope2 // 2)
    q = jnp.dot(lq, wq[...], preferred_element_type=jnp.float32)
    k = jnp.dot(lkv, wk[...], preferred_element_type=jnp.float32)
    v_s[:, tok] = lax.dot_general(wvt[...], lkv, NT, preferred_element_type=jnp.float32).astype(jnp.bfloat16)
    shared = rp.astype(jnp.float32)
    shared_sq = 0.5 * shared * shared
    lane = lax.broadcasted_iota(jnp.int32, (rows, rope2), 1)
    tqv, tkv = table[tok, :] * gq2, table[tok, :] * gk2
    for h in range(heads):
        for which in range(2):
            if which == 0:
                t1 = q[:, h * wide : h * wide + nope]
                t2 = q[:, h * wide + nope : (h + 1) * wide]
                sq, gain, turn, dest = t1 * t1 + 0.5 * t2 * t2, gq, tqv, q_s
            else:
                t1, t2 = k[:, h * nope : (h + 1) * nope], shared
                sq, gain, turn, dest = t1 * t1 + shared_sq, gk, tkv, k_s
            r = lax.rsqrt(jnp.sum(sq, axis=-1, keepdims=True) * inv + EPS)
            dest[h, tok, 0:nope] = (t1 * r * gain).astype(jnp.bfloat16)
            y = t2 * r * turn
            y = y + pltpu.roll(y, rope2 // 2, 1)
            if which == 1:
                y = jnp.where(lane < rope2 // 2, y, 0.0)
            dest[h, tok, nope:wide] = y.astype(jnp.bfloat16)


def attend_block(qb, rows, chunk, heads, vd, scale, q_s, k_s, v_s):
    qtok = pl.ds(pl.multiple_of(qb * rows, rows), rows)
    qs = [q_s[h, qtok, :] for h in range(heads)]
    factor = scale * LOG2E

    def step(kb, carry, masked):
        ktok = pl.ds(pl.multiple_of(kb * chunk, chunk), chunk)
        new = []
        for h in range(heads):
            m, l, acc = carry[h]
            s = lax.dot_general(k_s[h, ktok, :], qs[h], NT, preferred_element_type=jnp.float32) * factor
            if masked:
                kpos = kb * chunk + lax.broadcasted_iota(jnp.int32, (chunk, rows), 0)
                qpos = qb * rows + lax.broadcasted_iota(jnp.int32, (chunk, rows), 1)
                s = jnp.where(kpos <= qpos, s, NEG_BIG)
            m_new = jnp.maximum(m, jnp.max(s, axis=0, keepdims=True))
            alpha = jnp.exp2(m - m_new)
            p = jnp.exp2(s - m_new)
            l = l * alpha + jnp.sum(p, axis=0, keepdims=True)
            vt = v_s[h * vd : (h + 1) * vd, ktok]
            acc = acc * alpha + jnp.dot(vt, p.astype(jnp.bfloat16), preferred_element_type=jnp.float32)
            new.append((m_new, l, acc))
        return tuple(new)

    carry = tuple(
        (
            jnp.full((1, rows), NEG_BIG, jnp.float32),
            jnp.zeros((1, rows), jnp.float32),
            jnp.zeros((vd, rows), jnp.float32),
        )
        for _ in range(heads)
    )
    last = (qb * rows) // chunk
    carry = lax.fori_loop(0, last, lambda kb, c: step(kb, c, False), carry)
    carry = step(last, carry, True)
    return jnp.concatenate([jnp.transpose(acc / l) for _, l, acc in carry], axis=1).astype(jnp.bfloat16)


MESH = pl.DeviceIdType.MESH


class Links:
    def __init__(self, send_sems, recv_sems):
        self.send_sems, self.recv_sems, self.ids, self.sent = send_sems, recv_sems, {}, []

    def copy(self, role, src, dst, target):
        n = self.ids.setdefault(role, len(self.ids))
        return pltpu.make_async_remote_copy(
            src_ref=src, dst_ref=dst, send_sem=self.send_sems.at[n], recv_sem=self.recv_sems.at[n],
            device_id=target, device_id_type=MESH,
        )

    def send(self, role, src, dst, target, ok=None):
        self.sent.append((ok, role, src, dst, target))
        guard(ok, lambda: self.copy(role, src, dst, target).start())

    def arrive(self, role, dst, target, ok=None):
        guard(ok, lambda: self.copy(role, dst, dst, target).wait_recv())

    def drain(self):
        for ok, role, src, dst, target in self.sent:
            guard(ok, lambda: self.copy(role, src, dst, target).wait_send())
        self.sent = []


def guard(ok, action):
    if ok is None:
        action()
    else:
        pl.when(ok)(action)


def sem_count(nx, ny, nz, cores):
    gather = 5 * ((nx - 1) * cores + cores - 1) + 2 * (nx - 1) * (ny - 1) * cores
    latent = 2 * (2 * (nz - 1) + (2 * nz - 1) * (ny - 1))
    out = 2 * (nz - 1) + nz * (ny - 1) + nz * ny * (nx - 1) + nz * ny * nx * (cores - 1)
    return gather + latent + out


def layer_kernel(
    dims, chunk, heads, nope, vd, scale,
    tokens, in_gain, wqd, wld, wrope, q_lat_gain, kv_lat_gain, wqu, wku, wvu, q_gain, k_gain, table, out_gain, w_out,
    out,
    normed, wqd_g, wld_g, wqu_g, wku_g, wvu_g, w_g, wq_s, wvt, kvr_g, q_g, q_s, k_s, v_s, att_s, heads_g,
    send_sems, recv_sems, a2a_send, a2a_recv,
):
    nx, ny, nz, cores = dims
    seqs, dps = ny * nz, nx * cores
    rows = tokens.shape[0]
    kr = wld.shape[1]
    s, d = lax.axis_index("sp"), lax.axis_index("dp")
    y, z = lax.rem(s, ny), lax.div(s, ny)
    c, x = lax.rem(d, cores), lax.div(d, cores)
    links = Links(send_sems, recv_sems)

    def at_sp(target):
        return {"sp": target, "dp": d}

    def at_dp(target):
        return {"sp": s, "dp": target}

    barrier = pltpu.get_barrier_semaphore()
    for k in range(1, seqs):
        pl.semaphore_signal(barrier, inc=1, device_id=at_sp(lax.rem(s + k, seqs)), device_id_type=MESH)
    for k in range(1, dps):
        pl.semaphore_signal(barrier, inc=1, device_id=at_dp(lax.rem(d + k, dps)), device_id_type=MESH)
    pl.semaphore_wait(barrier, seqs + dps - 2)

    weights = ((wqd, wqd_g, True), (wld, wld_g, True), (wqu, wqu_g, False), (wku, wku_g, False), (wvu, wvu_g, False))

    def piece(ref, split, which):
        part = ref.shape[0] // ny
        return ref.at[pl.ds(pl.multiple_of(which * part, part), part)] if split else ref

    partners = [(dc, x * cores + lax.rem(c + dc, cores)) for dc in range(1, cores)]
    for a, (src, dst, split) in enumerate(weights):
        for dx in range(1, nx):
            target = lax.rem(x + dx, nx) * cores + c
            links.send(("x", a, dx), piece(src, split, y), piece(dst.at[d], split, y), at_dp(target))
        for dc, partner in partners:
            links.send(("c", a, dc), src, dst.at[d], at_dp(partner))

    part_out = w_out.shape[0]

    def w_block(zz, yy, xx, cc):
        first = ((zz * ny + yy) * dps + xx * cores + cc) * part_out
        return w_g.at[pl.ds(pl.multiple_of(first, part_out), part_out)]

    def w_z(way, step, src, dst, ok):
        links.send(("wz", way, step), src, dst, at_sp(jnp.clip(z + way, 0, nz - 1) * ny + y), ok)

    def w_z_step(step):
        for way in (1, -1):
            origin = z - way * (step + 1)
            ok = (origin >= 0) & (origin < nz)
            block = w_block(jnp.clip(origin, 0, nz - 1), y, x, c)
            links.arrive(("wz", way, step), block, at_sp(s), ok)
            if step < nz - 2:
                w_z(way, step + 1, block, block, ok & (z + way >= 0) & (z + way < nz))

    def w_x(k, dy):
        block = w_block(lax.rem(z + k, nz), lax.rem(y - dy + ny, ny), x, c)
        for dx in range(1, nx):
            links.send(("wx", k, dy, dx), block, block, at_dp(lax.rem(x + dx, nx) * cores + c))
        w_core(k, dy, 0, block)

    def w_core(k, dy, dx, block):
        for dc, partner in partners:
            links.send(("wc", k, dy, dx, dc), block, block, at_dp(partner))

    def w_x_arrive(k, dy):
        for dx in range(1, nx):
            block = w_block(lax.rem(z + k, nz), lax.rem(y - dy + ny, ny), lax.rem(x - dx + nx, nx), c)
            links.arrive(("wx", k, dy, dx), block, at_dp(d))
            w_core(k, dy, dx, block)

    for way in (1, -1):
        if nz > 1:
            w_z(way, 0, w_out, w_block(z, y, x, c), (z + way >= 0) & (z + way < nz))
    for src, dst, _ in weights:
        dst[d] = src[...]
    own_out = pl.ds(pl.multiple_of((s * dps + d) * part_out, part_out), part_out)
    w_g[own_out, :] = w_out[...]

    def norm(i, _):
        step = rows // 4
        band = pl.ds(pl.multiple_of(i * step, step), step)
        normed[band, :] = rms_scale(tokens[band, :].astype(jnp.float32), in_gain[...]).astype(jnp.bfloat16)
        return 0

    lax.fori_loop(0, 4, norm, 0)

    for a, (src, dst, split) in enumerate(weights):
        for dx in range(1, nx):
            origin = lax.rem(x - dx + nx, nx) * cores + c
            got = piece(dst.at[origin], split, y)
            links.arrive(("x", a, dx), got, at_dp(d))
            for dy in range(1, ny if split else 1):
                links.send(("y", a, dx, dy), got, got, at_sp(z * ny + lax.rem(y + dy, ny)))
            for dc, partner in partners:
                links.send(("cx", a, dx, dc), got, got, at_dp(partner))
    rope_key = jnp.dot(normed[...], wrope[...], preferred_element_type=jnp.float32)
    kvr_g[s, :, kr:] = with_swapped(rope_key).astype(jnp.bfloat16)
    for a, (src, dst, split) in enumerate(weights):
        for dx in range(1, nx):
            origin = lax.rem(x - dx + nx, nx) * cores + c
            for dy in range(1, ny if split else 1):
                got = piece(dst.at[origin], split, lax.rem(y - dy + ny, ny))
                links.arrive(("y", a, dx, dy), got, at_dp(d))
                for dc, partner in partners:
                    links.send(("cy", a, dx, dy, dc), got, got, at_dp(partner))

    def settle(a):
        src, dst, split = weights[a]
        for dc, _ in partners:
            other = lax.rem(c - dc + cores, cores)
            links.arrive(("c", a, dc), dst.at[x * cores + other], at_dp(d))
            for dx in range(1, nx):
                origin = dst.at[lax.rem(x - dx + nx, nx) * cores + other]
                links.arrive(("cx", a, dx, dc), piece(origin, split, y), at_dp(d))
                for dy in range(1, ny if split else 1):
                    got = piece(origin, split, lax.rem(y - dy + ny, ny))
                    links.arrive(("cy", a, dx, dy, dc), got, at_dp(d))

    def down(gathered):
        part = gathered.shape[1]
        total = None
        for k in range(dps):
            term = jnp.dot(
                normed[:, k * part : (k + 1) * part], gathered[k], preferred_element_type=jnp.float32
            )
            total = term if total is None else total + term
        return total

    buffers = (kvr_g, q_g)

    def over_y(b, tag, slot, ok=None):
        block = buffers[b].at[slot]
        for dy in range(1, ny):
            links.send(("ly", b, tag, dy), block, block, at_sp(z * ny + lax.rem(y + dy, ny)), ok)

    def along_z(b, way, step, slot, ok):
        block = buffers[b].at[slot]
        links.send(("z", b, way, step), block, block, at_sp(jnp.clip(z + way, 0, nz - 1) * ny + y), ok)

    def launch(b):
        over_y(b, 0, s)
        for way in (1, -1):
            if nz > 1:
                along_z(b, way, 0, s, (z + way >= 0) & (z + way < nz))

    if nz > 1:
        w_z_step(0)
    settle(1)
    kvr_g[s, :, :kr] = rms_scale(down(wld_g), kv_lat_gain[...]).astype(jnp.bfloat16)
    launch(0)
    settle(0)
    q_g[s] = rms_scale(down(wqd_g), q_lat_gain[...]).astype(jnp.bfloat16)
    launch(1)
    for step in range(1, nz - 1):
        w_z_step(step)
    for k in range(nz):
        w_x(k, 0)

    for step in range(nz - 1):
        for b in range(2):
            for way in (1, -1):
                origin = z - way * (step + 1)
                ok = (origin >= 0) & (origin < nz)
                slot = jnp.clip(origin, 0, nz - 1) * ny + y
                links.arrive(("z", b, way, step), buffers[b].at[slot], at_sp(s), ok)
                if step < nz - 2:
                    along_z(b, way, step + 1, slot, ok & (z + way >= 0) & (z + way < nz))
                over_y(b, way * (step + 1), slot, ok)
    for k in range(nz):
        for dy in range(1, ny):
            block = w_block(lax.rem(z + k, nz), y, x, c)
            links.send(("wy", k, dy), block, block, at_sp(z * ny + lax.rem(y + dy, ny)))
    settle(2)
    settle(3)
    settle(4)
    wk_full = wku_g.reshape(dps * wku.shape[0], wku.shape[1])
    for k in range(dps):
        depth = wqu.shape[0]
        up = wqu_g[k].astype(jnp.float32)
        columns = []
        for h in range(heads):
            head = up[:, h * (wqu.shape[1] // heads) : (h + 1) * (wqu.shape[1] // heads)]
            columns += [head[:, :nope], with_swapped(head[:, nope:])]
        wq_s[k * depth : (k + 1) * depth, :] = jnp.concatenate(columns, axis=1).astype(jnp.bfloat16)
    wv_full = wvu_g.reshape(dps * wvu.shape[0], wvu.shape[1])
    wvt[...] = jnp.transpose(wv_full[...].astype(jnp.float32)).astype(jnp.bfloat16)
    gq, gk = q_gain[:, :nope], k_gain[:, :nope]
    gq2, gk2 = with_swapped(q_gain[:, nope:]), with_swapped(k_gain[:, nope:])
    for b in range(2):
        for tag in range(1 - nz, nz):
            zz = z - tag
            ok = None if tag == 0 else (zz >= 0) & (zz < nz)
            for dy in range(1, ny):
                slot = jnp.clip(zz, 0, nz - 1) * ny + lax.rem(y - dy + ny, ny)
                links.arrive(("ly", b, tag, dy), buffers[b].at[slot], at_sp(s), ok)

    def project(i, _):
        project_block(
            i, rows, heads, nope, vd, q_g[i], kvr_g[i, :, :kr], kvr_g[i, :, kr:],
            wq_s, wk_full, wvt, gq, gk, gq2, gk2, table, q_s, k_s, v_s,
        )
        return 0

    lax.fori_loop(0, seqs, project, 0)

    def hand_over(qb):
        return pltpu.make_async_remote_copy(
            src_ref=att_s.at[qb], dst_ref=heads_g.at[s], send_sem=a2a_send.at[qb],
            recv_sem=a2a_recv.at[s], device_id=at_sp(qb), device_id_type=MESH,
        )

    def attend(i, _):
        qb = lax.rem(s + 1 + i, seqs)
        att_s[qb] = attend_block(qb, rows, chunk, heads, vd, scale, q_s, k_s, v_s)

        @pl.when(i < seqs - 1)
        def _():
            hand_over(qb).start()

        return 0

    lax.fori_loop(0, seqs // 2, attend, 0)
    for k in range(nz):
        for dy in range(1, ny):
            block = w_block(lax.rem(z + k, nz), lax.rem(y - dy + ny, ny), x, c)
            links.arrive(("wy", k, dy), block, at_sp(s))
            w_x(k, dy)
    for k in range(nz):
        w_x_arrive(k, 0)
    lax.fori_loop(seqs // 2, seqs, attend, 0)
    for k in range(nz):
        for dy in range(1, ny):
            w_x_arrive(k, dy)
    heads_g[s] = att_s[s]
    for k in range(1, seqs):
        origin = lax.rem(s + k, seqs)
        pltpu.make_async_remote_copy(
            src_ref=att_s.at[origin], dst_ref=heads_g.at[origin], send_sem=a2a_send.at[origin],
            recv_sem=a2a_recv.at[origin], device_id=at_sp(origin), device_id_type=MESH,
        ).wait()
    width = heads * vd
    square = jnp.zeros((rows, 1), jnp.float32)
    for k in range(seqs):
        block = heads_g[k].astype(jnp.float32)
        square = square + jnp.sum(block * block, axis=-1, keepdims=True)
    r = lax.rsqrt(square * (1.0 / (seqs * width)) + EPS)
    for k in range(seqs):
        cols = slice(k * width, (k + 1) * width)
        normed[:, cols] = (heads_g[k].astype(jnp.float32) * r * out_gain[:, cols]).astype(jnp.bfloat16)
    for k in range(nz):
        for dy in range(ny):
            for dx in range(nx):
                for dc, _ in partners:
                    block = w_block(
                        lax.rem(z + k, nz), lax.rem(y - dy + ny, ny), lax.rem(x - dx + nx, nx),
                        lax.rem(c - dc + cores, cores),
                    )
                    links.arrive(("wc", k, dy, dx, dc), block, at_dp(d))
    tile = 256 if out.shape[1] % 256 == 0 else out.shape[1]

    def project_out(i, _):
        cols = pl.ds(pl.multiple_of(i * tile, tile), tile)
        out[:, cols] = jnp.dot(normed[...], w_g[:, cols], preferred_element_type=jnp.float32).astype(out.dtype)
        return 0

    lax.fori_loop(0, out.shape[1] // tile, project_out, 0)
    links.drain()


def per_device(
    tokens, in_gain, w_query_down, w_latent_down, w_rope_key, query_latent_gain, latent_gain,
    w_query_up, w_key_up, w_value_up, query_gain, key_gain, out_gain, w_out,
):
    seqs, dps = lax.axis_size("sp"), lax.axis_size("dp")
    cores = 2 if dps % 2 == 0 else 1
    nx = dps // cores
    ny = nx if seqs % nx == 0 else 1
    nz = seqs // ny
    heads = HEADS // seqs
    own_rows = tokens.shape[1]
    length = own_rows * seqs
    rope = w_rope_key.shape[1]
    nope = w_key_up.shape[1] // heads
    vd = w_value_up.shape[1] // heads
    wide = nope + 2 * rope
    chunk = min(2 * own_rows, length)
    sems = sem_count(nx, ny, nz, cores)
    b16 = jnp.bfloat16

    def gathered(w):
        return pltpu.VMEM((dps,) + w.shape, b16)

    result = pl.pallas_call(
        functools.partial(
            layer_kernel, (nx, ny, nz, cores), chunk, heads, nope, vd, float(nope + rope) ** -0.5
        ),
        out_shape=jax.ShapeDtypeStruct((own_rows, w_out.shape[1]), b16),
        in_specs=[pl.BlockSpec(memory_space=pltpu.VMEM)] * 15,
        out_specs=pl.BlockSpec(memory_space=pltpu.VMEM),
        scratch_shapes=[
            pltpu.VMEM((own_rows, max(tokens.shape[2], w_out.shape[0] * seqs * dps)), b16),
            gathered(w_query_down), gathered(w_latent_down), gathered(w_query_up), gathered(w_key_up), gathered(w_value_up),
            pltpu.VMEM((w_out.shape[0] * seqs * dps, w_out.shape[1]), b16),
            pltpu.VMEM((w_query_down.shape[1], heads * wide), b16),
            pltpu.VMEM((heads * vd, w_latent_down.shape[1]), b16),
            pltpu.VMEM((seqs, own_rows, w_latent_down.shape[1] + 2 * rope), b16),
            pltpu.VMEM((seqs, own_rows, w_query_down.shape[1]), b16),
            pltpu.VMEM((heads, length, wide), b16),
            pltpu.VMEM((heads, length, wide), b16),
            pltpu.VMEM((heads * vd, length), b16),
            pltpu.VMEM((seqs, own_rows, heads * vd), b16),
            pltpu.VMEM((seqs, own_rows, heads * vd), b16),
            pltpu.SemaphoreType.DMA((sems,)),
            pltpu.SemaphoreType.DMA((sems,)),
            pltpu.SemaphoreType.DMA((seqs,)),
            pltpu.SemaphoreType.DMA((seqs,)),
        ],
        compiler_params=pltpu.CompilerParams(
            vmem_limit_bytes=56 * 1024 * 1024, collective_id=0, has_side_effects=True
        ),
        cost_estimate=pl.CostEstimate(flops=60 * 10**9, bytes_accessed=10**8, transcendentals=5 * 10**6),
    )(
        tokens.reshape(own_rows, tokens.shape[2]), in_gain[None], w_query_down, w_latent_down, w_rope_key,
        query_latent_gain[None], latent_gain[None], w_query_up, w_key_up, w_value_up,
        query_gain[None], key_gain[None], jnp.asarray(rotation_table(length, rope)), out_gain[None], w_out,
    )
    return result.reshape(1, own_rows, w_out.shape[1])


def solution(mesh):
    in_specs = (
        P("dp", "sp", None), P(), P("dp", None), P("dp", None), P(), P(), P(),
        P("dp", "sp"), P("dp", "sp"), P("dp", "sp"), P(), P(), P(), P(("sp", "dp"), None),
    )
    return jax.shard_map(
        per_device, mesh=mesh, in_specs=in_specs, out_specs=P("dp", "sp", None), check_vma=False
    )
```

profile of v0, /device:TPU:1, one launch (start us, length us, event | category | flops | bytes accessed | tf_op | source)
XLA Modules:
  0.0 132.3 jit_solution(1645479321639968264)
XLA Ops:
  0.0 2.0 %copy.16.wrope = bf16[2048,64]{1,0:T(8,128)(2,1)} copy(bf16[2048,64]{0,1:T(8,128)(2,1)} %param.19) | data formatting | bytes 524288 | tf_op args[4]
  2.0 128.0 %shard_map.145 = bf16[256,2048]{1,0:T(8,128)(2,1)} custom-call(bf16[256,2048]{1,0:T(8,128)(2,1)} %bitcast.9, f32[1,2048]{1,0:T(1,128)} %bitcast.10, bf16[512,512]{1,0:T(8,128)(2,1)} %wqd.1, bf16[512,256]{1,0:T(8,128)(2,1)} %wld.1, bf16[2048,64]{1,0:T(8,128)(2,1)} %copy.16.wrope, f32[1,512]{1,0:T(1,128)} %bitcast.12, f32[1,256]{1,0:T(1,128)} %bitcast.13, ...), custom_call_target="tpu_custom_call" | custom-call | flops 60000002048 | bytes 100000000 | tf_op jit(solution)/shard_map/pallas_call | solution.py:448
  129.9 2.3 %copy.18 = bf16[1,256,2048]{2,1,0:T(8,128)(2,1)} copy(bf16[1,256,2048]{2,1,0:T(8,128)(2,1)} %bitcast.8) | data formatting | bytes 2097152
where the time goes:
time: 132 us
  Pallas kernels  128 us (97%)
  local copies, waits for them, and re-layouts  4.26 us (3%)
    pallas_call x1, Pallas kernels, per_device(): pl.pallas_call(functools.partial(layer_kernel, (nx, ny, nz, cores), chunk...  128 us
    unnamed x2, local copies, waits for them, and re-layouts  4.26 us

commit v1 on v0

v1 whole, which is shorter than its diff:
```python
import functools

import jax
import jax.numpy as jnp
import numpy as np
from jax import lax
from jax.experimental import pallas as pl
from jax.experimental.pallas import tpu as pltpu
from jax.sharding import PartitionSpec as P

HEADS = 16
EPS = 1e-06
THETA = 10000.0
NEG_BIG = -1e30
LOG2E = 1.4426950408889634
NT = (((1,), (1,)), ((), ()))


def rms_scale(values, scaling):
    return values * lax.rsqrt(jnp.mean(values * values, axis=-1, keepdims=True) + EPS) * scaling


def swap_halves(x):
    half = x.shape[-1] // 2
    return jnp.concatenate([x[..., half:], x[..., :half]], axis=-1)


def rotation_table(length, width):
    half = width // 2
    frequency = np.float32(THETA) ** (-np.arange(half, dtype=np.float32) / np.float32(half))
    angles = np.arange(length, dtype=np.float32)[:, None] * frequency[None, :]
    cosine, sine = np.cos(angles), np.sin(angles)
    return np.concatenate([cosine, cosine, -sine, sine], axis=-1).astype(np.float32)


def with_swapped(x):
    return jnp.concatenate([x, swap_halves(x)], axis=-1)


def head_finish(t1, t2, r, gain, turn):
    rope2 = t2.shape[1]
    y = t2 * r * turn
    return (t1 * r * gain).astype(jnp.bfloat16), y + pltpu.roll(y, rope2 // 2, 1)


def project_queries(rows, heads, nope, lq, wq, gain, turn, q_s):
    wide = wq.shape[1] // heads
    rope2 = wide - nope
    inv = 1.0 / (nope + rope2 // 2)
    q = jnp.dot(lq, wq[...], preferred_element_type=jnp.float32)
    for h in range(heads):
        t1 = q[:, h * wide : h * wide + nope]
        t2 = q[:, h * wide + nope : (h + 1) * wide]
        r = lax.rsqrt(jnp.sum(t1 * t1 + 0.5 * t2 * t2, axis=-1, keepdims=True) * inv + EPS)
        first, last = head_finish(t1, t2, r, gain, turn)
        q_s[h, :, 0:nope] = first
        q_s[h, :, nope:wide] = last.astype(jnp.bfloat16)


def pack_rope(rope_key):
    part = rope_key.shape[0] // 4
    band = [rope_key[g * part : (g + 1) * part] for g in range(4)]
    return jnp.concatenate(band, axis=1).astype(jnp.bfloat16)


def unpack_rope(packed, rope2):
    quarter = rope2 // 4
    lane = lax.broadcasted_iota(jnp.int32, (packed.shape[0], rope2), 1)
    bands = []
    for g in range(4):
        p = packed[:, (g // 2) * rope2 : (g // 2 + 1) * rope2].astype(jnp.float32)
        if g % 2 == 0:
            front, b, a = p, pltpu.roll(p, quarter, 1), pltpu.roll(p, 3 * quarter, 1)
        else:
            front, b, a = pltpu.roll(p, 2 * quarter, 1), pltpu.roll(p, 3 * quarter, 1), pltpu.roll(p, quarter, 1)
        bands.append(jnp.where(lane < 2 * quarter, front, jnp.where(lane < 3 * quarter, b, a)))
    return jnp.concatenate(bands, axis=0)


def project_keys(block, rows, nope, lkv, shared, wks, wvt, gain, turn, k_s, v_s):
    tok = pl.ds(pl.multiple_of(block * rows, rows), rows)
    rope2 = shared.shape[1]
    wide = nope + rope2
    inv = 1.0 / (nope + rope2 // 2)
    v_s[:, tok] = lax.dot_general(wvt[...], lkv, NT, preferred_element_type=jnp.float32).astype(jnp.bfloat16)
    half_sq = 0.5 * shared * shared
    lane = lax.broadcasted_iota(jnp.int32, (rows, rope2), 1)
    turned = shared * turn
    turned = turned + pltpu.roll(turned, rope2 // 2, 1)
    turned = jnp.where(lane < rope2 // 2, turned, 0.0)
    h = 0
    for wk in wks:
        k = jnp.dot(lkv, wk, preferred_element_type=jnp.float32)
        for j in range(k.shape[1] // nope):
            t1 = k[:, j * nope : (j + 1) * nope]
            r = lax.rsqrt(jnp.sum(t1 * t1 + half_sq, axis=-1, keepdims=True) * inv + EPS)
            k_s[h, tok, 0:nope] = (t1 * r * gain).astype(jnp.bfloat16)
            k_s[h, tok, nope:wide] = (turned * r).astype(jnp.bfloat16)
            h += 1


def attend_block(qb, rows, chunk, heads, vd, scale, q_s, k_s, v_s):
    qs = [q_s[h] for h in range(heads)]
    factor = scale * LOG2E

    def step(kb, carry, masked):
        ktok = pl.ds(pl.multiple_of(kb * chunk, chunk), chunk)
        new = []
        for h in range(heads):
            m, l, acc = carry[h]
            s = lax.dot_general(k_s[h, ktok, :], qs[h], NT, preferred_element_type=jnp.float32) * factor
            if masked:
                kpos = kb * chunk + lax.broadcasted_iota(jnp.int32, (chunk, rows), 0)
                qpos = qb * rows + lax.broadcasted_iota(jnp.int32, (chunk, rows), 1)
                s = jnp.where(kpos <= qpos, s, NEG_BIG)
            m_new = jnp.maximum(m, jnp.max(s, axis=0, keepdims=True))
            alpha = jnp.exp2(m - m_new)
            p = jnp.exp2(s - m_new)
            l = l * alpha + jnp.sum(p, axis=0, keepdims=True)
            vt = v_s[h * vd : (h + 1) * vd, ktok]
            acc = acc * alpha + jnp.dot(vt, p.astype(jnp.bfloat16), preferred_element_type=jnp.float32)
            new.append((m_new, l, acc))
        return tuple(new)

    carry = tuple(
        (
            jnp.full((1, rows), NEG_BIG, jnp.float32),
            jnp.zeros((1, rows), jnp.float32),
            jnp.zeros((vd, rows), jnp.float32),
        )
        for _ in range(heads)
    )
    last = (qb * rows) // chunk
    carry = lax.fori_loop(0, last, lambda kb, c: step(kb, c, False), carry)
    carry = step(last, carry, True)
    return jnp.concatenate([jnp.transpose(acc / l) for _, l, acc in carry], axis=1).astype(jnp.bfloat16)


MESH = pl.DeviceIdType.MESH


class Links:
    def __init__(self, send_sems, recv_sems, send_rows, recv_rows):
        self.send_sems, self.recv_sems, self.ids, self.sent = send_sems, recv_sems, {}, []
        self.send_rows, self.recv_rows, self.row_ids = send_rows, recv_rows, {}

    def sems(self, role, at):
        if at is None:
            n = self.ids.setdefault(role, len(self.ids))
            return self.send_sems.at[n], self.recv_sems.at[n]
        n = self.row_ids.setdefault(role, len(self.row_ids))
        return self.send_rows.at[n, at], self.recv_rows.at[n, at]

    def copy(self, role, at, src, dst, target, land=None):
        send, recv = self.sems(role, at)
        if land is not None:
            recv = self.sems(role, land)[1]
        return pltpu.make_async_remote_copy(
            src_ref=src, dst_ref=dst, send_sem=send, recv_sem=recv, device_id=target, device_id_type=MESH,
        )

    def send(self, role, src, dst, target, ok=None, at=None):
        self.sent.append((ok, role, at, src, dst, target))
        guard(ok, lambda: self.copy(role, at, src, dst, target).start())

    def arrive(self, role, dst, target, ok=None, at=None):
        guard(ok, lambda: self.copy(role, at, dst, dst, target).wait_recv())

    def drain(self):
        for ok, role, at, src, dst, target in self.sent:
            guard(ok, lambda: self.copy(role, at, src, dst, target).wait_send())
        self.sent = []


def guard(ok, action):
    if ok is None:
        action()
    else:
        pl.when(ok)(action)


DOWN_CUTS = (1, 2)


def sem_counts(nx, ny, nz, cores):
    items = sum(DOWN_CUTS)
    over, pair = nx - 1, cores - 1
    down = items * over * ny * (1 + pair) + 2 * pair
    up = 3 * (over + (ny - 1) + over * (ny - 1) + nx * ny * pair)
    rows = 2 + (ny - 1) + 2 + 1 + 2 + (ny - 1) + ny * over + ny * nx * pair
    return down + up, rows


def layer_kernel(
    dims, chunk, heads, nope, vd, scale,
    tokens, in_gain, wqd, wld, wrope, q_lat_gain, kv_lat_gain, wqu, wku, wvu, q_gain, k_gain, table, out_gain, w_out,
    out,
    normed, wqd_g, wld_g, wqu_g, wku_g, wvu_g, w_g, wq_s, wvt, kv_g, q_g, q_s, k_s, v_s, att_s, heads_g,
    send_sems, recv_sems, send_rows, recv_rows,
):
    nx, ny, nz, cores = dims
    seqs, dps = ny * nz, nx * cores
    rows = tokens.shape[0]
    s, d = lax.axis_index("sp"), lax.axis_index("dp")
    y, z = lax.rem(s, ny), lax.div(s, ny)
    c, x = lax.rem(d, cores), lax.div(d, cores)
    links = Links(send_sems, recv_sems, send_rows, recv_rows)

    def at_sp(target):
        return {"sp": target, "dp": d}

    def at_dp(target):
        return {"sp": s, "dp": target}

    def at_z(target):
        return at_sp(target * ny + y)

    def at_y(step):
        return at_sp(z * ny + lax.rem(y + step, ny))

    def at_x(step):
        return at_dp(lax.rem(x + step, nx) * cores + c)

    def at_core(step):
        return at_dp(x * cores + lax.rem(c + step, cores))

    def back_y(step):
        return lax.rem(y - step + ny, ny)

    def back_x(step):
        return lax.rem(x - step + nx, nx)

    def back_core(step):
        return lax.rem(c - step + cores, cores)

    barrier = pltpu.get_barrier_semaphore()
    peers = [at_z(lax.rem(z + k, nz)) for k in range(1, nz)] + [at_y(k) for k in range(1, ny)]
    peers += [at_x(k) for k in range(1, nx)] + [at_core(k) for k in range(1, cores)]
    for peer in peers:
        pl.semaphore_signal(barrier, inc=1, device_id=peer, device_id_type=MESH)
    pl.semaphore_wait(barrier, len(peers))

    xs, ys, cs = range(1, nx), range(1, ny), range(1, cores)

    downs = ((wld, wld_g, DOWN_CUTS[0]), (wqd, wqd_g, DOWN_CUTS[1]))
    items = [(a, cut) for a in range(2) for cut in range(downs[a][2])]

    def piece(ref, a, cut, which):
        cuts = downs[a][2]
        part = ref.shape[0] // (ny * cuts)
        return ref.at[pl.ds(pl.multiple_of((which * cuts + cut) * part, part), part)]

    for it, (a, cut) in enumerate(items):
        src, dst, _ = downs[a]
        for dx in xs:
            links.send(("x", it, dx), piece(src, a, cut, y), piece(dst.at[d], a, cut, y), at_x(dx))
    for a, (src, dst, _) in enumerate(downs):
        for dc in cs:
            links.send(("c", a, dc), src, dst.at[d], at_core(dc))

    ups = ((wqu, wqu_g), (wku, wku_g), (wvu, wvu_g))
    for a, (src, dst) in enumerate(ups):
        for dy in ys:
            links.send(("uy", a, dy), src, dst.at[y, d], at_y(dy))
        for dx in xs:
            links.send(("ux", a, dx), src, dst.at[y, d], at_x(dx))
        for dc in cs:
            links.send(("uc", a, 0, 0, dc), src, dst.at[y, d], at_core(dc))

    part_out = w_out.shape[0]

    def w_block(zz, yy, xx, cc):
        first = ((zz * ny + yy) * dps + xx * cores + cc) * part_out
        return w_g.at[pl.ds(pl.multiple_of(first, part_out), part_out)]

    def along_z(role, way, origin, src, dst, ok):
        links.send((role, way), src, dst, at_z(jnp.clip(z + way, 0, nz - 1)), ok, at=origin)

    def z_arrival(step, way):
        origin = z - way * (step + 1)
        ok = (origin >= 0) & (origin < nz)
        return jnp.clip(origin, 0, nz - 1), ok, ok & (z + way >= 0) & (z + way < nz)

    def w_over_y(origin, src, ok):
        for dy in ys:
            links.send(("wy", dy), src, w_block(origin, y, x, c), at_y(dy), ok, at=origin)

    def w_over_x(origin, dyo, src, ok):
        for dx in xs:
            links.send(("wx", dyo, dx), src, w_block(origin, back_y(dyo), x, c), at_x(dx), ok, at=origin)

    def w_over_core(origin, dyo, dxo, src, ok):
        for dc in cs:
            dst = w_block(origin, back_y(dyo), back_x(dxo), c)
            links.send(("wc", dyo, dxo, dc), src, dst, at_core(dc), ok, at=origin)

    def w_z_arrive(step):
        for way in (1, -1):
            origin, ok, _ = z_arrival(step, way)
            block = w_block(origin, y, x, c)
            links.arrive(("wz", way), block, at_sp(s), ok, at=origin)
            w_over_x(origin, 0, block, ok)
            w_over_core(origin, 0, 0, block, ok)

    def w_z_relay(step):
        for way in (1, -1):
            origin, _, more = z_arrival(step, way)
            block = w_block(origin, y, x, c)
            along_z("wz", way, origin, block, block, more)

    def w_y_send(step):
        for way in (1, -1):
            origin, ok, _ = z_arrival(step, way)
            w_over_y(origin, w_block(origin, y, x, c), ok)

    def w_y_arrive_at(origin, ok):
        for dy in ys:
            block = w_block(origin, back_y(dy), x, c)
            links.arrive(("wy", dy), block, at_sp(s), ok, at=origin)
            w_over_x(origin, dy, block, ok)
            w_over_core(origin, dy, 0, block, ok)

    def w_y_arrive(step):
        for way in (1, -1):
            origin, ok, _ = z_arrival(step, way)
            w_y_arrive_at(origin, ok)

    def w_x_arrive(origin, dyo):
        for dx in xs:
            block = w_block(origin, back_y(dyo), back_x(dx), c)
            links.arrive(("wx", dyo, dx), block, at_dp(d), at=origin)
            w_over_core(origin, dyo, dx, block, None)

    own_block = w_block(z, y, x, c)
    for way in (1, -1):
        if nz > 1:
            along_z("wz", way, z, w_out, own_block, (z + way >= 0) & (z + way < nz))
    w_over_x(z, 0, w_out, None)
    w_over_core(z, 0, 0, w_out, None)

    for src, dst, _ in downs:
        dst[d] = src[...]
    for src, dst in ups:
        dst[y, d] = src[...]
    own_out = pl.ds(pl.multiple_of((s * dps + d) * part_out, part_out), part_out)
    w_g[own_out, :] = w_out[...]

    def norm(i, _):
        step = rows // 4
        band = pl.ds(pl.multiple_of(i * step, step), step)
        normed[band, :] = rms_scale(tokens[band, :].astype(jnp.float32), in_gain[...]).astype(jnp.bfloat16)
        return 0

    lax.fori_loop(0, 4, norm, 0)
    rope_key = lax.dot_general(normed[...], wrope[...], NT, preferred_element_type=jnp.float32)
    kv_g[s, rows:, :] = pack_rope(rope_key)

    def down_x(it):
        a, cut = items[it]
        dst = downs[a][1]
        for dx in xs:
            got = piece(dst.at[back_x(dx) * cores + c], a, cut, y)
            links.arrive(("x", it, dx), got, at_dp(d))
            for dy in ys:
                links.send(("y", it, dx, dy), got, got, at_y(dy))
            for dc in cs:
                links.send(("cx", it, dx, dc), got, got, at_core(dc))

    def down_y(it):
        a, cut = items[it]
        dst = downs[a][1]
        for dx in xs:
            for dy in ys:
                got = piece(dst.at[back_x(dx) * cores + c], a, cut, back_y(dy))
                links.arrive(("y", it, dx, dy), got, at_dp(d))
                for dc in cs:
                    links.send(("cy", it, dx, dy, dc), got, got, at_core(dc))

    def settle_down(a):
        dst = downs[a][1]
        for dc in cs:
            links.arrive(("c", a, dc), dst.at[x * cores + back_core(dc)], at_dp(d))
            for it in range(len(items)):
                if items[it][0] != a:
                    continue
                for dx in xs:
                    origin = dst.at[back_x(dx) * cores + back_core(dc)]
                    links.arrive(("cx", it, dx, dc), piece(origin, a, items[it][1], y), at_dp(d))
                    for dy in ys:
                        got = piece(origin, a, items[it][1], back_y(dy))
                        links.arrive(("cy", it, dx, dy, dc), got, at_dp(d))

    def down(gathered):
        part = gathered.shape[1]
        total = None
        for k in range(dps):
            term = jnp.dot(normed[:, k * part : (k + 1) * part], gathered[k], preferred_element_type=jnp.float32)
            total = term if total is None else total + term
        return total

    def kv_over_y(zz, ok=None):
        block = kv_g.at[zz * ny + y]
        for dy in ys:
            links.send(("kvy", dy), block, block, at_y(dy), ok, at=zz)

    def launch(role, block):
        for way in (1, -1):
            if nz > 1:
                along_z(role, way, z, block, block, (z + way >= 0) & (z + way < nz))

    down_x(0)
    down_x(1)
    down_y(0)
    if nz > 1:
        w_z_arrive(0)
        w_z_relay(0)
    for it in range(2, len(items)):
        down_x(it)
    settle_down(0)
    kv_g[s, :rows, :] = rms_scale(down(wld_g), kv_lat_gain[...]).astype(jnp.bfloat16)
    launch("kv", kv_g.at[s])
    kv_over_y(z)
    for it in range(1, len(items)):
        down_y(it)

    def up_spread(a):
        dst = ups[a][1]
        for dy in ys:
            got = dst.at[back_y(dy), d]
            links.arrive(("uy", a, dy), got, at_dp(d))
            for dc in cs:
                links.send(("uc", a, dy, 0, dc), got, got, at_core(dc))
        for dx in xs:
            got = dst.at[y, back_x(dx) * cores + c]
            links.arrive(("ux", a, dx), got, at_dp(d))
            for dy in ys:
                links.send(("uxy", a, dx, dy), got, got, at_y(dy))
            for dc in cs:
                links.send(("uc", a, 0, dx, dc), got, got, at_core(dc))

    def up_diagonal(a):
        dst = ups[a][1]
        for dx in xs:
            for dy in ys:
                got = dst.at[back_y(dy), back_x(dx) * cores + c]
                links.arrive(("uxy", a, dx, dy), got, at_dp(d))
                for dc in cs:
                    links.send(("uc", a, dy, dx, dc), got, got, at_core(dc))

    def settle_up(a):
        dst = ups[a][1]
        for dy in range(ny):
            for dx in range(nx):
                for dc in cs:
                    got = dst.at[back_y(dy), back_x(dx) * cores + back_core(dc)]
                    links.arrive(("uc", a, dy, dx, dc), got, at_dp(d))

    settle_down(1)
    q_g[z] = rms_scale(down(wqd_g), q_lat_gain[...]).astype(jnp.bfloat16)
    launch("q", q_g.at[z])

    def z_relay(role, step, buffer, after=None):
        for way in (1, -1):
            origin, ok, more = z_arrival(step, way)
            block = buffer(origin)
            links.arrive((role, way), block, at_sp(s), ok, at=origin)
            along_z(role, way, origin, block, block, more)
            if after is not None:
                after(origin, ok)

    def kv_block(zz):
        return kv_g.at[zz * ny + y]

    for a in range(3):
        up_spread(a)
    if nz > 1:
        z_relay("kv", 0, kv_block, kv_over_y)
    for a in range(3):
        up_diagonal(a)
    for a in range(3):
        settle_up(a)
    shard_heads = heads // ny
    depth = wqu.shape[0]
    for yy in range(ny):
        for k in range(dps):
            up = wqu_g[yy, k].astype(jnp.float32)
            width = wqu.shape[1] // shard_heads
            for h in range(shard_heads):
                head = up[:, h * width : (h + 1) * width]
                both = jnp.concatenate([head[:, :nope], with_swapped(head[:, nope:])], axis=1)
                wide = both.shape[1]
                first = (yy * shard_heads + h) * wide
                wq_s[k * depth : (k + 1) * depth, first : first + wide] = both.astype(jnp.bfloat16)
        wv = wvu_g[yy].reshape(dps * wvu.shape[0], wvu.shape[1])
        wvt[yy * shard_heads * vd : (yy + 1) * shard_heads * vd, :] = jnp.transpose(
            wv.astype(jnp.float32)
        ).astype(jnp.bfloat16)
    gq, gk = q_gain[:, :nope], k_gain[:, :nope]
    gq2, gk2 = with_swapped(q_gain[:, nope:]), with_swapped(k_gain[:, nope:])
    rope2 = gq2.shape[1]

    def project_kv(block):
        tok = pl.ds(pl.multiple_of(block * rows, rows), rows)
        wks = [wku_g[yy].reshape(dps * wku.shape[0], wku.shape[1]) for yy in range(ny)]
        shared = unpack_rope(kv_g[block, rows:, :], rope2)
        project_keys(block, rows, nope, kv_g[block, :rows, :], shared, wks, wvt, gk, table[tok, :] * gk2, k_s, v_s)

    def near(i):
        m = jnp.minimum(z, nz - 1 - z)
        two = i <= 2 * m
        dist = jnp.where(two, lax.div(i + 1, 2), i - m)
        up = jnp.where(two, lax.rem(i, 2) == 1, z < nz - 1 - z)
        return jnp.where(up, z + dist, z - dist)

    def kv_column(zz):
        def one(j, _):
            yy = lax.rem(y + j, ny)
            project_kv(zz * ny + yy)
            return 0

        for dy in ys:
            links.arrive(("kvy", dy), kv_g.at[zz * ny + back_y(dy)], at_sp(s), at=zz)
        lax.fori_loop(0, ny, one, 0)

    def kv_columns(first, last):
        def one(i, _):
            kv_column(near(i))
            return 0

        lax.fori_loop(first, last, one, 0)

    kv_columns(0, 1)
    for step in range(1, nz - 1):
        z_relay("kv", step, kv_block, kv_over_y)
        if step < nz - 2:
            w_z_arrive(step)
        z_relay("q", step - 1, lambda zz: q_g.at[zz])
    for step in range(1, nz - 2):
        w_z_relay(step)
    w_over_y(z, w_out, None)
    for step in range(nz - 1):
        if step < nz - 2:
            w_y_send(step)
    kv_columns(1, nz)
    if nz > 1:
        z_relay("q", nz - 2, lambda zz: q_g.at[zz])

    def hand_over(zz):
        return links.copy("a2a", zz, att_s.at[zz], heads_g.at[z], at_z(zz), land=z)

    def attend(i, _):
        zz = near(lax.rem(i + 1, nz))
        qb = zz * ny + y
        tok = pl.ds(pl.multiple_of(qb * rows, rows), rows)
        project_queries(rows, heads, nope, q_g[zz], wq_s, gq, table[tok, :] * gq2, q_s)
        att_s[zz] = attend_block(qb, rows, chunk, heads, vd, scale, q_s, k_s, v_s)

        @pl.when(i < nz - 1)
        def _():
            hand_over(zz).start()

        return 0

    def attend_range(first, last):
        lax.fori_loop(first, last, attend, 0)

    cuts = [(k * nz) // 4 for k in range(5)]
    attend_range(cuts[0], cuts[1])
    w_y_arrive_at(z, None)
    attend_range(cuts[1], cuts[2])
    if nz > 1:
        w_y_arrive(0)
        w_z_arrive(nz - 2) if nz > 2 else None
        w_y_send(nz - 2)
    attend_range(cuts[2], cuts[3])
    for step in range(1, nz - 2):
        w_y_arrive(step)
    for k in range(nz):
        w_x_arrive(lax.rem(z + k, nz), 0)
    attend_range(cuts[3], cuts[4])
    if nz > 1:
        for step in range(max(nz - 2, 1), nz - 1):
            w_y_arrive(step)
    for k in range(nz):
        for dy in ys:
            w_x_arrive(lax.rem(z + k, nz), dy)
    heads_g[z] = att_s[z]
    for k in range(1, nz):
        origin = lax.rem(z + k, nz)
        links.copy("a2a", origin, att_s.at[origin], heads_g.at[z], at_z(origin), land=origin).wait_send()
        links.copy("a2a", origin, heads_g.at[origin], heads_g.at[origin], at_z(origin), land=origin).wait_recv()
    width = heads * vd
    square = jnp.zeros((rows, 1), jnp.float32)
    for k in range(nz):
        block = heads_g[k].astype(jnp.float32)
        square = square + jnp.sum(block * block, axis=-1, keepdims=True)
    r = lax.rsqrt(square * (1.0 / (nz * width)) + EPS)
    for k in range(nz):
        cols = slice(k * width, (k + 1) * width)
        normed[:, cols] = (heads_g[k].astype(jnp.float32) * r * out_gain[:, cols]).astype(jnp.bfloat16)
    for k in range(nz):
        origin = lax.rem(z + k, nz)
        for dy in range(ny):
            for dx in range(nx):
                for dc in cs:
                    block = w_block(origin, back_y(dy), back_x(dx), back_core(dc))
                    links.arrive(("wc", dy, dx, dc), block, at_dp(d), at=origin)
    tile = 256 if out.shape[1] % 256 == 0 else out.shape[1]

    def project_out(i, _):
        cols = pl.ds(pl.multiple_of(i * tile, tile), tile)
        out[:, cols] = jnp.dot(normed[...], w_g[:, cols], preferred_element_type=jnp.float32).astype(out.dtype)
        return 0

    lax.fori_loop(0, out.shape[1] // tile, project_out, 0)
    links.drain()


def per_device(
    tokens, in_gain, w_query_down, w_latent_down, w_rope_key, query_latent_gain, latent_gain,
    w_query_up, w_key_up, w_value_up, query_gain, key_gain, out_gain, w_out,
):
    seqs, dps = lax.axis_size("sp"), lax.axis_size("dp")
    cores = 2 if dps % 2 == 0 else 1
    nx = dps // cores
    ny = nx if seqs % nx == 0 else 1
    nz = seqs // ny
    heads = HEADS // nz
    own_rows = tokens.shape[1]
    length = own_rows * seqs
    rope = w_rope_key.shape[1]
    nope = w_key_up.shape[1] * ny // heads
    vd = w_value_up.shape[1] * ny // heads
    wide = nope + 2 * rope
    chunk = min(2 * own_rows, length)
    sems, sem_rows = sem_counts(nx, ny, nz, cores)
    b16 = jnp.bfloat16

    def gathered(w, *lead):
        return pltpu.VMEM(lead + (dps,) + w.shape, b16)

    result = pl.pallas_call(
        functools.partial(
            layer_kernel, (nx, ny, nz, cores), chunk, heads, nope, vd, float(nope + rope) ** -0.5
        ),
        out_shape=jax.ShapeDtypeStruct((own_rows, w_out.shape[1]), b16),
        in_specs=[pl.BlockSpec(memory_space=pltpu.VMEM)] * 15,
        out_specs=pl.BlockSpec(memory_space=pltpu.VMEM),
        scratch_shapes=[
            pltpu.VMEM((own_rows, max(tokens.shape[2], w_out.shape[0] * seqs * dps)), b16),
            gathered(w_query_down), gathered(w_latent_down),
            gathered(w_query_up, ny), gathered(w_key_up, ny), gathered(w_value_up, ny),
            pltpu.VMEM((w_out.shape[0] * seqs * dps, w_out.shape[1]), b16),
            pltpu.VMEM((w_query_down.shape[1], heads * wide), b16),
            pltpu.VMEM((heads * vd, w_latent_down.shape[1]), b16),
            pltpu.VMEM((seqs, own_rows + own_rows * rope // w_latent_down.shape[1], w_latent_down.shape[1]), b16),
            pltpu.VMEM((nz, own_rows, w_query_down.shape[1]), b16),
            pltpu.VMEM((heads, own_rows, wide), b16),
            pltpu.VMEM((heads, length, wide), b16),
            pltpu.VMEM((heads * vd, length), b16),
            pltpu.VMEM((nz, own_rows, heads * vd), b16),
            pltpu.VMEM((nz, own_rows, heads * vd), b16),
            pltpu.SemaphoreType.DMA((sems,)),
            pltpu.SemaphoreType.DMA((sems,)),
            pltpu.SemaphoreType.DMA((sem_rows, nz)),
            pltpu.SemaphoreType.DMA((sem_rows, nz)),
        ],
        compiler_params=pltpu.CompilerParams(
            vmem_limit_bytes=56 * 1024 * 1024, collective_id=0, has_side_effects=True
        ),
        cost_estimate=pl.CostEstimate(flops=60 * 10**9, bytes_accessed=10**8, transcendentals=5 * 10**6),
    )(
        tokens.reshape(own_rows, tokens.shape[2]), in_gain[None], w_query_down, w_latent_down, w_rope_key.T,
        query_latent_gain[None], latent_gain[None], w_query_up, w_key_up, w_value_up,
        query_gain[None], key_gain[None], jnp.asarray(rotation_table(length, rope)), out_gain[None], w_out,
    )
    return result.reshape(1, own_rows, w_out.shape[1])


def solution(mesh):
    in_specs = (
        P("dp", "sp", None), P(), P("dp", None), P("dp", None), P(), P(), P(),
        P("dp", "sp"), P("dp", "sp"), P("dp", "sp"), P(), P(), P(), P(("sp", "dp"), None),
    )
    return jax.shard_map(
        per_device, mesh=mesh, in_specs=in_specs, out_specs=P("dp", "sp", None), check_vma=False
    )
```

time: 132 us -> 100 us (0.76)
  the two profiles are of different devices: /device:TPU:1 before, /device:TPU:25 now
where the time goes in v1:
time: 100 us
  Pallas kernels  97.8 us (98%)
  local copies, waits for them, and re-layouts  2.3 us (2%)
    pallas_call x1, Pallas kernels, per_device(): pl.pallas_call(functools.partial(layer_kernel, (nx, ny, nz, cores), chunk...  97.8 us
    unnamed x1, local copies, waits for them, and re-layouts  2.3 us

profile of v1, /device:TPU:25, one launch (start us, length us, event | category | flops | bytes accessed | tf_op | source)
XLA Modules:
  0.0 100.1 jit_solution(10664953756547703843)
XLA Ops:
  0.0 97.8 %shard_map.145 = bf16[256,2048]{1,0:T(8,128)(2,1)} custom-call(bf16[256,2048]{1,0:T(8,128)(2,1)} %bitcast.10, f32[1,2048]{1,0:T(1,128)} %bitcast.12, bf16[512,512]{1,0:T(8,128)(2,1)} %wqd.1, bf16[512,256]{1,0:T(8,128)(2,1)} %wld.1, bf16[64,2048]{1,0:T(8,128)(2,1)} %bitcast.11, f32[1,512]{1,0:T(1,128)} %bitcast.14, f32[1,256]{1,0:T(1,128)} %bitcast.15, ...), custom_call_target="tpu_custom_call" | custom-call | flops 60000002048 | bytes 100000000 | tf_op jit(solution)/shard_map/pallas_call | solution.py:642
  97.8 2.3 %copy.17 = bf16[1,256,2048]{2,1,0:T(8,128)(2,1)} copy(bf16[1,256,2048]{2,1,0:T(8,128)(2,1)} %bitcast.9) | data formatting | bytes 2097152

commit v2 on v1

--- a/solution.py
+++ b/solution.py
@@ -99,41 +99,62 @@
             h += 1
 
 
-def attend_block(qb, rows, chunk, heads, vd, scale, q_s, k_s, v_s):
-    qs = [q_s[h] for h in range(heads)]
+def attend_item(j, y, rows, chunk, heads, vd, scale, masked, q_s, k_s, v_s, m_s, l_s, acc_s, scores):
+    ktok = pl.ds(pl.multiple_of(j * chunk, chunk), chunk)
     factor = scale * LOG2E
-
-    def step(kb, carry, masked):
-        ktok = pl.ds(pl.multiple_of(kb * chunk, chunk), chunk)
-        new = []
-        for h in range(heads):
-            m, l, acc = carry[h]
-            s = lax.dot_general(k_s[h, ktok, :], qs[h], NT, preferred_element_type=jnp.float32) * factor
-            if masked:
-                kpos = kb * chunk + lax.broadcasted_iota(jnp.int32, (chunk, rows), 0)
-                qpos = qb * rows + lax.broadcasted_iota(jnp.int32, (chunk, rows), 1)
-                s = jnp.where(kpos <= qpos, s, NEG_BIG)
-            m_new = jnp.maximum(m, jnp.max(s, axis=0, keepdims=True))
-            alpha = jnp.exp2(m - m_new)
-            p = jnp.exp2(s - m_new)
-            l = l * alpha + jnp.sum(p, axis=0, keepdims=True)
-            vt = v_s[h * vd : (h + 1) * vd, ktok]
-            acc = acc * alpha + jnp.dot(vt, p.astype(jnp.bfloat16), preferred_element_type=jnp.float32)
-            new.append((m_new, l, acc))
-        return tuple(new)
-
-    carry = tuple(
-        (
-            jnp.full((1, rows), NEG_BIG, jnp.float32),
-            jnp.zeros((1, rows), jnp.float32),
-            jnp.zeros((vd, rows), jnp.float32),
+    sub = 128
+
+    def product(h):
+        scores[h] = lax.dot_general(k_s[h, ktok, :], q_s[h], NT, preferred_element_type=jnp.float32)
+
+    def band(h, first):
+        s = scores[h, first : first + sub, :]
+        if masked:
+            kpos = first + lax.broadcasted_iota(jnp.int32, (sub, rows), 0)
+            qpos = y * rows + lax.broadcasted_iota(jnp.int32, (sub, rows), 1)
+            s = jnp.where(kpos <= qpos, s, NEG_BIG)
+        return s
+
+    product(0)
+    for h in range(heads):
+        if h + 1 < heads:
+            product(h + 1)
+        top = None
+        for first in range(0, chunk, sub):
+            part = jnp.max(band(h, first).reshape(sub // 8, 8, rows), axis=0)
+            top = part if top is None else jnp.maximum(top, part)
+        m = m_s[h]
+        m_new = jnp.maximum(m, jnp.max(top, axis=0, keepdims=True) * factor)
+        alpha = jnp.exp2(m - m_new)
+        total, weights = None, []
+        for first in range(0, chunk, sub):
+            p = jnp.exp2(band(h, first) * factor - m_new)
+            part = jnp.sum(p.reshape(sub // 8, 8, rows), axis=0)
+            total = part if total is None else total + part
+            weights.append(p.astype(jnp.bfloat16))
+        m_s[h] = m_new
+        l_s[h] = l_s[h] * alpha + jnp.sum(total, axis=0, keepdims=True)
+        vt = v_s[h * vd : (h + 1) * vd, ktok]
+        acc_s[h] = acc_s[h] * alpha + jnp.dot(
+            vt, jnp.concatenate(weights, axis=0), preferred_element_type=jnp.float32
         )
-        for _ in range(heads)
-    )
-    last = (qb * rows) // chunk
-    carry = lax.fori_loop(0, last, lambda kb, c: step(kb, c, False), carry)
-    carry = step(last, carry, True)
-    return jnp.concatenate([jnp.transpose(acc / l) for _, l, acc in carry], axis=1).astype(jnp.bfloat16)
+
+
+def attend_block(i, y, rows, chunk, heads, vd, scale, q_s, k_s, v_s, m_s, l_s, acc_s, scores):
+    m_s[...] = jnp.full(m_s.shape, NEG_BIG, jnp.float32)
+    l_s[...] = jnp.zeros(l_s.shape, jnp.float32)
+    acc_s[...] = jnp.zeros(acc_s.shape, jnp.float32)
+
+    def item(j, masked):
+        attend_item(j, y, rows, chunk, heads, vd, scale, masked, q_s, k_s, v_s, m_s, l_s, acc_s, scores)
+
+    def step(j, _):
+        item(j, False)
+        return 0
+
+    lax.fori_loop(0, i, step, 0)
+    item(i, True)
+    return jnp.concatenate([jnp.transpose(acc_s[h] / l_s[h]) for h in range(heads)], axis=1).astype(jnp.bfloat16)
 
 
 MESH = pl.DeviceIdType.MESH
@@ -186,7 +207,7 @@
     items = sum(DOWN_CUTS)
     over, pair = nx - 1, cores - 1
     down = items * over * ny * (1 + pair) + 2 * pair
-    up = 3 * (over + (ny - 1) + over * (ny - 1) + nx * ny * pair)
+    up = 3 * (over * ny + (ny - 1) + nx * ny * pair)
     rows = 2 + (ny - 1) + 2 + 1 + 2 + (ny - 1) + ny * over + ny * nx * pair
     return down + up, rows
 
@@ -195,7 +216,7 @@
     dims, chunk, heads, nope, vd, scale,
     tokens, in_gain, wqd, wld, wrope, q_lat_gain, kv_lat_gain, wqu, wku, wvu, q_gain, k_gain, table, out_gain, w_out,
     out,
-    normed, wqd_g, wld_g, wqu_g, wku_g, wvu_g, w_g, wq_s, wvt, kv_g, q_g, q_s, k_s, v_s, att_s, heads_g,
+    normed, wqd_g, wld_g, wqu_g, wku_g, wvu_g, w_g, wq_s, wvt, kv_g, q_g, q_s, k_s, v_s, m_s, l_s, acc_s, scores, att_s, heads_g,
     send_sems, recv_sems, send_rows, recv_rows,
 ):
     nx, ny, nz, cores = dims
@@ -233,6 +254,13 @@
     def back_core(step):
         return lax.rem(c - step + cores, cores)
 
+    def near(i):
+        m = jnp.minimum(z, nz - 1 - z)
+        two = i <= 2 * m
+        dist = jnp.where(two, lax.div(i + 1, 2), i - m)
+        up = jnp.where(two, lax.rem(i, 2) == 1, z < nz - 1 - z)
+        return jnp.where(up, z + dist, z - dist)
+
     barrier = pltpu.get_barrier_semaphore()
     peers = [at_z(lax.rem(z + k, nz)) for k in range(1, nz)] + [at_y(k) for k in range(1, ny)]
     peers += [at_x(k) for k in range(1, nx)] + [at_core(k) for k in range(1, cores)]
@@ -262,8 +290,6 @@
     for a, (src, dst) in enumerate(ups):
         for dy in ys:
             links.send(("uy", a, dy), src, dst.at[y, d], at_y(dy))
-        for dx in xs:
-            links.send(("ux", a, dx), src, dst.at[y, d], at_x(dx))
         for dc in cs:
             links.send(("uc", a, 0, 0, dc), src, dst.at[y, d], at_core(dc))
 
@@ -294,36 +320,44 @@
             dst = w_block(origin, back_y(dyo), back_x(dxo), c)
             links.send(("wc", dyo, dxo, dc), src, dst, at_core(dc), ok, at=origin)
 
-    def w_z_arrive(step):
+    def w_z_relay(step, onward=True):
+        for way in (1, -1):
+            origin, ok, more = z_arrival(step, way)
+            block = w_block(origin, y, x, c)
+            links.arrive(("wz", way), block, at_sp(s), ok, at=origin)
+            if onward:
+                along_z("wz", way, origin, block, block, more)
+
+    def w_z_onward(step):
+        for way in (1, -1):
+            origin, ok, more = z_arrival(step, way)
+            block = w_block(origin, y, x, c)
+            along_z("wz", way, origin, block, block, more)
+
+    def w_z_spread(step):
         for way in (1, -1):
             origin, ok, _ = z_arrival(step, way)
             block = w_block(origin, y, x, c)
-            links.arrive(("wz", way), block, at_sp(s), ok, at=origin)
             w_over_x(origin, 0, block, ok)
             w_over_core(origin, 0, 0, block, ok)
 
-    def w_z_relay(step):
-        for way in (1, -1):
-            origin, _, more = z_arrival(step, way)
-            block = w_block(origin, y, x, c)
-            along_z("wz", way, origin, block, block, more)
-
-    def w_y_send(step):
-        for way in (1, -1):
-            origin, ok, _ = z_arrival(step, way)
-            w_over_y(origin, w_block(origin, y, x, c), ok)
-
-    def w_y_arrive_at(origin, ok):
+    def w_y_near(k):
+        origin = near(k)
+        w_over_y(origin, w_block(origin, y, x, c), None)
+
+    def w_y_copies(origin):
+        copies = []
         for dy in ys:
             block = w_block(origin, back_y(dy), x, c)
-            links.arrive(("wy", dy), block, at_sp(s), ok, at=origin)
-            w_over_x(origin, dy, block, ok)
-            w_over_core(origin, dy, 0, block, ok)
-
-    def w_y_arrive(step):
-        for way in (1, -1):
-            origin, ok, _ = z_arrival(step, way)
-            w_y_arrive_at(origin, ok)
+            copies += [links.copy(("wx", dy, dx), origin, block, block, at_x(dx)) for dx in xs]
+            copies += [links.copy(("wc", dy, 0, dc), origin, block, block, at_core(dc)) for dc in cs]
+        return copies
+
+    def w_y_service(origin):
+        for dy in ys:
+            links.arrive(("wy", dy), w_block(origin, back_y(dy), x, c), at_sp(s), at=origin)
+        for copy in w_y_copies(origin):
+            copy.start()
 
     def w_x_arrive(origin, dyo):
         for dx in xs:
@@ -335,8 +369,6 @@
     for way in (1, -1):
         if nz > 1:
             along_z("wz", way, z, w_out, own_block, (z + way >= 0) & (z + way < nz))
-    w_over_x(z, 0, w_out, None)
-    w_over_core(z, 0, 0, w_out, None)
 
     for src, dst, _ in downs:
         dst[d] = src[...]
@@ -409,13 +441,22 @@
                 along_z(role, way, z, block, block, (z + way >= 0) & (z + way < nz))
 
     down_x(0)
+    if nz > 1:
+        w_z_relay(0)
     down_x(1)
     down_y(0)
-    if nz > 1:
-        w_z_arrive(0)
-        w_z_relay(0)
     for it in range(2, len(items)):
         down_x(it)
+    for a, (src, dst) in enumerate(ups):
+        for dx in xs:
+            links.send(("ux", a, 0, dx), src, dst.at[y, d], at_x(dx))
+        for dy in ys:
+            got = dst.at[back_y(dy), d]
+            links.arrive(("uy", a, dy), got, at_dp(d))
+            for dx in xs:
+                links.send(("ux", a, dy, dx), got, got, at_x(dx))
+            for dc in cs:
+                links.send(("uc", a, dy, 0, dc), got, got, at_core(dc))
     settle_down(0)
     kv_g[s, :rows, :] = rms_scale(down(wld_g), kv_lat_gain[...]).astype(jnp.bfloat16)
     launch("kv", kv_g.at[s])
@@ -425,25 +466,10 @@
 
     def up_spread(a):
         dst = ups[a][1]
-        for dy in ys:
-            got = dst.at[back_y(dy), d]
-            links.arrive(("uy", a, dy), got, at_dp(d))
-            for dc in cs:
-                links.send(("uc", a, dy, 0, dc), got, got, at_core(dc))
-        for dx in xs:
-            got = dst.at[y, back_x(dx) * cores + c]
-            links.arrive(("ux", a, dx), got, at_dp(d))
-            for dy in ys:
-                links.send(("uxy", a, dx, dy), got, got, at_y(dy))
-            for dc in cs:
-                links.send(("uc", a, 0, dx, dc), got, got, at_core(dc))
-
-    def up_diagonal(a):
-        dst = ups[a][1]
-        for dx in xs:
-            for dy in ys:
+        for dy in range(ny):
+            for dx in xs:
                 got = dst.at[back_y(dy), back_x(dx) * cores + c]
-                links.arrive(("uxy", a, dx, dy), got, at_dp(d))
+                links.arrive(("ux", a, dy, dx), got, at_dp(d))
                 for dc in cs:
                     links.send(("uc", a, dy, dx, dc), got, got, at_core(dc))
 
@@ -457,13 +483,12 @@
 
     settle_down(1)
     q_g[z] = rms_scale(down(wqd_g), q_lat_gain[...]).astype(jnp.bfloat16)
-    launch("q", q_g.at[z])
-
-    def z_relay(role, step, buffer, after=None):
+
+    def z_relay(role, step, buffer, after=None, lazy=False):
         for way in (1, -1):
             origin, ok, more = z_arrival(step, way)
             block = buffer(origin)
-            links.arrive((role, way), block, at_sp(s), ok, at=origin)
+            links.arrive((role, way), block, at_sp(s), more if lazy else ok, at=origin)
             along_z(role, way, origin, block, block, more)
             if after is not None:
                 after(origin, ok)
@@ -475,8 +500,10 @@
         up_spread(a)
     if nz > 1:
         z_relay("kv", 0, kv_block, kv_over_y)
-    for a in range(3):
-        up_diagonal(a)
+    w_over_x(z, 0, w_out, None)
+    w_over_core(z, 0, 0, w_out, None)
+    if nz > 1:
+        w_z_spread(0)
     for a in range(3):
         settle_up(a)
     shard_heads = heads // ny
@@ -505,13 +532,6 @@
         shared = unpack_rope(kv_g[block, rows:, :], rope2)
         project_keys(block, rows, nope, kv_g[block, :rows, :], shared, wks, wvt, gk, table[tok, :] * gk2, k_s, v_s)
 
-    def near(i):
-        m = jnp.minimum(z, nz - 1 - z)
-        two = i <= 2 * m
-        dist = jnp.where(two, lax.div(i + 1, 2), i - m)
-        up = jnp.where(two, lax.rem(i, 2) == 1, z < nz - 1 - z)
-        return jnp.where(up, z + dist, z - dist)
-
     def kv_column(zz):
         def one(j, _):
             yy = lax.rem(y + j, ny)
@@ -529,60 +549,67 @@
 
         lax.fori_loop(first, last, one, 0)
 
+
+    def q_block(zz):
+        return q_g.at[zz]
+
+    for step in range(1, nz - 2):
+        z_relay("kv", step, kv_block, kv_over_y)
+    launch("q", q_g.at[z])
     kv_columns(0, 1)
-    for step in range(1, nz - 1):
+    for step in range(max(nz - 2, 1), nz - 1):
         z_relay("kv", step, kv_block, kv_over_y)
-        if step < nz - 2:
-            w_z_arrive(step)
-        z_relay("q", step - 1, lambda zz: q_g.at[zz])
     for step in range(1, nz - 2):
-        w_z_relay(step)
+        w_z_relay(step, False)
+        w_z_spread(step)
+        z_relay("q", step - 1, q_block, lazy=True)
+    for step in range(1, nz - 2):
+        w_z_onward(step)
     w_over_y(z, w_out, None)
-    for step in range(nz - 1):
-        if step < nz - 2:
-            w_y_send(step)
+    for k in range(1, nz - 1):
+        w_y_near(k)
     kv_columns(1, nz)
-    if nz > 1:
-        z_relay("q", nz - 2, lambda zz: q_g.at[zz])
+    w_y_service(z)
 
     def hand_over(zz):
         return links.copy("a2a", zz, att_s.at[zz], heads_g.at[z], at_z(zz), land=z)
 
     def attend(i, _):
-        zz = near(lax.rem(i + 1, nz))
+        zz = near(i)
+        low = zz < z
+        last = jnp.where(low, z == nz - 1, z == 0)
+        for way, side in ((1, low), (-1, zz > z)):
+            links.arrive(("q", way), q_g.at[zz], at_sp(s), side & last, at=zz)
         qb = zz * ny + y
         tok = pl.ds(pl.multiple_of(qb * rows, rows), rows)
         project_queries(rows, heads, nope, q_g[zz], wq_s, gq, table[tok, :] * gq2, q_s)
-        att_s[zz] = attend_block(qb, rows, chunk, heads, vd, scale, q_s, k_s, v_s)
-
-        @pl.when(i < nz - 1)
+        att_s[zz] = attend_block(zz, y, rows, chunk, heads, vd, scale, q_s, k_s, v_s, m_s, l_s, acc_s, scores)
+
+        @pl.when(i > 0)
         def _():
             hand_over(zz).start()
+        @pl.when((i > 0) & (i < nz - 2))
+        def _():
+            w_y_service(near(i + 1))
 
         return 0
 
-    def attend_range(first, last):
-        lax.fori_loop(first, last, attend, 0)
-
-    cuts = [(k * nz) // 4 for k in range(5)]
-    attend_range(cuts[0], cuts[1])
-    w_y_arrive_at(z, None)
-    attend_range(cuts[1], cuts[2])
+    lax.fori_loop(0, 1, attend, 0)
     if nz > 1:
-        w_y_arrive(0)
-        w_z_arrive(nz - 2) if nz > 2 else None
-        w_y_send(nz - 2)
-    attend_range(cuts[2], cuts[3])
-    for step in range(1, nz - 2):
-        w_y_arrive(step)
+        w_y_service(near(1))
+    for step in range(1, nz - 1):
+        z_relay("q", step, q_block, lazy=True)
+    for step in range(max(nz - 2, 1), nz - 1):
+        w_z_relay(step, False)
+        w_z_spread(step)
+    if nz > 2:
+        w_y_near(nz - 1)
+    lax.fori_loop(1, max(nz - 1, 1), attend, 0)
+    if nz > 2:
+        w_y_service(near(nz - 1))
+    lax.fori_loop(max(nz - 1, 1), nz, attend, 0)
     for k in range(nz):
-        w_x_arrive(lax.rem(z + k, nz), 0)
-    attend_range(cuts[3], cuts[4])
-    if nz > 1:
-        for step in range(max(nz - 2, 1), nz - 1):
-            w_y_arrive(step)
-    for k in range(nz):
-        for dy in ys:
+        for dy in range(ny):
             w_x_arrive(lax.rem(z + k, nz), dy)
     heads_g[z] = att_s[z]
     for k in range(1, nz):
@@ -613,6 +640,9 @@
         return 0
 
     lax.fori_loop(0, out.shape[1] // tile, project_out, 0)
+    for k in range(nz):
+        for copy in w_y_copies(lax.rem(z + k, nz)):
+            copy.wait_send()
     links.drain()
 
 
@@ -632,7 +662,7 @@
     nope = w_key_up.shape[1] * ny // heads
     vd = w_value_up.shape[1] * ny // heads
     wide = nope + 2 * rope
-    chunk = min(2 * own_rows, length)
+    chunk = ny * own_rows
     sems, sem_rows = sem_counts(nx, ny, nz, cores)
     b16 = jnp.bfloat16
 
@@ -658,6 +688,10 @@
             pltpu.VMEM((heads, own_rows, wide), b16),
             pltpu.VMEM((heads, length, wide), b16),
             pltpu.VMEM((heads * vd, length), b16),
+            pltpu.VMEM((heads, 1, own_rows), jnp.float32),
+            pltpu.VMEM((heads, 1, own_rows), jnp.float32),
+            pltpu.VMEM((heads, vd, own_rows), jnp.float32),
+            pltpu.VMEM((heads, chunk, own_rows), jnp.float32),
             pltpu.VMEM((nz, own_rows, heads * vd), b16),
             pltpu.VMEM((nz, own_rows, heads * vd), b16),
             pltpu.SemaphoreType.DMA((sems,)),

time: 100 us -> 91.9 us (0.919)
  the two profiles are of different devices: /device:TPU:25 before, /device:TPU:0 now
where the time goes in v2:
time: 91.9 us; the launch traced here: 91.7 us
  Pallas kernels  89.4 us (97%)
  local copies, waits for them, and re-layouts  2.3 us (3%)
    pallas_call x1, Pallas kernels, per_device(): pl.pallas_call(functools.partial(layer_kernel, (nx, ny, nz, cores), chunk...  89.4 us
    unnamed x1, local copies, waits for them, and re-layouts  2.3 us

profile of v2, /device:TPU:0, one launch (start us, length us, event | category | flops | bytes accessed | tf_op | source)
XLA Modules:
  0.0 91.7 jit_solution(9004774573912463182)
XLA Ops:
  0.0 89.4 %shard_map.145 = bf16[256,2048]{1,0:T(8,128)(2,1)} custom-call(bf16[256,2048]{1,0:T(8,128)(2,1)} %bitcast.10, f32[1,2048]{1,0:T(1,128)} %bitcast.12, bf16[512,512]{1,0:T(8,128)(2,1)} %wqd.1, bf16[512,256]{1,0:T(8,128)(2,1)} %wld.1, bf16[64,2048]{1,0:T(8,128)(2,1)} %bitcast.11, f32[1,512]{1,0:T(1,128)} %bitcast.14, f32[1,256]{1,0:T(1,128)} %bitcast.15, ...), custom_call_target="tpu_custom_call" | custom-call | flops 60000002048 | bytes 100000000 | tf_op jit(solution)/shard_map/pallas_call | solution.py:672
  89.4 2.3 %copy.17 = bf16[1,256,2048]{2,1,0:T(8,128)(2,1)} copy(bf16[1,256,2048]{2,1,0:T(8,128)(2,1)} %bitcast.9) | data formatting | bytes 2097152

commit v3 on v2

--- a/solution.py
+++ b/solution.py
@@ -99,16 +99,19 @@
             h += 1
 
 
-def attend_item(j, y, rows, chunk, heads, vd, scale, masked, q_s, k_s, v_s, m_s, l_s, acc_s, scores):
+def attend_item(j, y, rows, chunk, heads, vd, scale, masked, q_s, k_s, v_s, m_s, l_s, work):
     ktok = pl.ds(pl.multiple_of(j * chunk, chunk), chunk)
     factor = scale * LOG2E
     sub = 128
 
+    def score_rows(h, first=0, count=chunk):
+        return pl.ds(heads * vd + (h % 2) * chunk + first, count)
+
     def product(h):
-        scores[h] = lax.dot_general(k_s[h, ktok, :], q_s[h], NT, preferred_element_type=jnp.float32)
+        work[score_rows(h), :] = lax.dot_general(k_s[h, ktok, :], q_s[h], NT, preferred_element_type=jnp.float32)
 
     def band(h, first):
-        s = scores[h, first : first + sub, :]
+        s = work[score_rows(h, first, sub), :]
         if masked:
             kpos = first + lax.broadcasted_iota(jnp.int32, (sub, rows), 0)
             qpos = y * rows + lax.broadcasted_iota(jnp.int32, (sub, rows), 1)
@@ -135,18 +138,19 @@
         m_s[h] = m_new
         l_s[h] = l_s[h] * alpha + jnp.sum(total, axis=0, keepdims=True)
         vt = v_s[h * vd : (h + 1) * vd, ktok]
-        acc_s[h] = acc_s[h] * alpha + jnp.dot(
+        own = pl.ds(h * vd, vd)
+        work[own, :] = work[own, :] * alpha + jnp.dot(
             vt, jnp.concatenate(weights, axis=0), preferred_element_type=jnp.float32
         )
 
 
-def attend_block(i, y, rows, chunk, heads, vd, scale, q_s, k_s, v_s, m_s, l_s, acc_s, scores):
+def attend_block(i, y, rows, chunk, heads, vd, scale, q_s, k_s, v_s, m_s, l_s, work):
     m_s[...] = jnp.full(m_s.shape, NEG_BIG, jnp.float32)
     l_s[...] = jnp.zeros(l_s.shape, jnp.float32)
-    acc_s[...] = jnp.zeros(acc_s.shape, jnp.float32)
+    work[0 : heads * vd, :] = jnp.zeros((heads * vd, rows), jnp.float32)
 
     def item(j, masked):
-        attend_item(j, y, rows, chunk, heads, vd, scale, masked, q_s, k_s, v_s, m_s, l_s, acc_s, scores)
+        attend_item(j, y, rows, chunk, heads, vd, scale, masked, q_s, k_s, v_s, m_s, l_s, work)
 
     def step(j, _):
         item(j, False)
@@ -154,7 +158,7 @@
 
     lax.fori_loop(0, i, step, 0)
     item(i, True)
-    return jnp.concatenate([jnp.transpose(acc_s[h] / l_s[h]) for h in range(heads)], axis=1).astype(jnp.bfloat16)
+    return jnp.concatenate([jnp.transpose(work[h * vd : (h + 1) * vd, :] / l_s[h]) for h in range(heads)], axis=1).astype(jnp.bfloat16)
 
 
 MESH = pl.DeviceIdType.MESH
@@ -201,14 +205,16 @@
 
 
 DOWN_CUTS = (1, 2)
-
-
-def sem_counts(nx, ny, nz, cores):
+TURNED = 2
+
+
+def sem_counts(nx, ny, nz, cores, group):
     items = sum(DOWN_CUTS)
     over, pair = nx - 1, cores - 1
     down = items * over * ny * (1 + pair) + 2 * pair
-    up = 3 * (over * ny + (ny - 1) + nx * ny * pair)
-    rows = 2 + (ny - 1) + 2 + 1 + 2 + (ny - 1) + ny * over + ny * nx * pair
+    nzs = nz // group
+    up = 3 * (nzs - 1 + nzs * (ny - 1) + nzs * ny * over + nzs * ny * nx * pair)
+    rows = 2 + (ny - 1) + (group - 1) + 1 + 2 + (ny - 1) + ny * over + ny * nx * pair + over * (ny - 1)
     return down + up, rows
 
 
@@ -216,15 +222,17 @@
     dims, chunk, heads, nope, vd, scale,
     tokens, in_gain, wqd, wld, wrope, q_lat_gain, kv_lat_gain, wqu, wku, wvu, q_gain, k_gain, table, out_gain, w_out,
     out,
-    normed, wqd_g, wld_g, wqu_g, wku_g, wvu_g, w_g, wq_s, wvt, kv_g, q_g, q_s, k_s, v_s, m_s, l_s, acc_s, scores, att_s, heads_g,
+    normed, wqd_g, wld_g, wqu_g, wku_g, wvu_g, w_g, wq_s, wvt, kv_g, q_g, q_s, k_s, v_s, m_s, l_s, work, att_s, heads_g,
     send_sems, recv_sems, send_rows, recv_rows,
 ):
-    nx, ny, nz, cores = dims
+    nx, ny, nz, cores, group = dims
     seqs, dps = ny * nz, nx * cores
     rows = tokens.shape[0]
     s, d = lax.axis_index("sp"), lax.axis_index("dp")
     y, z = lax.rem(s, ny), lax.div(s, ny)
     c, x = lax.rem(d, cores), lax.div(d, cores)
+    zl, zo = lax.rem(z, group), lax.div(z, group)
+    zb, nzs = z - zl, nz // group
     links = Links(send_sems, recv_sems, send_rows, recv_rows)
 
     def at_sp(target):
@@ -268,7 +276,7 @@
         pl.semaphore_signal(barrier, inc=1, device_id=peer, device_id_type=MESH)
     pl.semaphore_wait(barrier, len(peers))
 
-    xs, ys, cs = range(1, nx), range(1, ny), range(1, cores)
+    xs, ys, cs, zs = range(1, nx), range(1, ny), range(1, cores), range(1, nzs)
 
     downs = ((wld, wld_g, DOWN_CUTS[0]), (wqd, wqd_g, DOWN_CUTS[1]))
     items = [(a, cut) for a in range(2) for cut in range(downs[a][2])]
@@ -287,11 +295,30 @@
             links.send(("c", a, dc), src, dst.at[d], at_core(dc))
 
     ups = ((wqu, wqu_g), (wku, wku_g), (wvu, wvu_g))
+    def up_slot(k, dy, dx, cc):
+        return lax.rem(zo - k + nzs, nzs), back_y(dy), back_x(dx) * cores + cc
+
+    def up_over_x(a, k, dy, src):
+        dst = ups[a][1].at[up_slot(k, dy, 0, c)]
+        for dx in xs:
+            links.send(("ux", a, k, dy, dx), src, dst, at_x(dx))
+
+    def up_over_y(a, k, src):
+        dst = ups[a][1].at[up_slot(k, 0, 0, c)]
+        for dy in ys:
+            links.send(("uy", a, k, dy), src, dst, at_y(dy))
+
+    def up_over_core(a, k, dy, dx, src):
+        dst = ups[a][1].at[up_slot(k, dy, dx, c)]
+        for dc in cs:
+            links.send(("uc", a, k, dy, dx, dc), src, dst, at_core(dc))
+
     for a, (src, dst) in enumerate(ups):
-        for dy in ys:
-            links.send(("uy", a, dy), src, dst.at[y, d], at_y(dy))
-        for dc in cs:
-            links.send(("uc", a, 0, 0, dc), src, dst.at[y, d], at_core(dc))
+        for k in zs:
+            links.send(("uz", a, k), src, dst.at[zo, y, d], at_z(lax.rem(z + k * group, nz)))
+        up_over_y(a, 0, src)
+        up_over_x(a, 0, 0, src)
+        up_over_core(a, 0, 0, 0, src)
 
     part_out = w_out.shape[0]
 
@@ -345,19 +372,35 @@
         origin = near(k)
         w_over_y(origin, w_block(origin, y, x, c), None)
 
-    def w_y_copies(origin):
+    def w_y_copies(origin, turned):
         copies = []
         for dy in ys:
             block = w_block(origin, back_y(dy), x, c)
-            copies += [links.copy(("wx", dy, dx), origin, block, block, at_x(dx)) for dx in xs]
+            if not turned:
+                copies += [links.copy(("wx", dy, dx), origin, block, block, at_x(dx)) for dx in xs]
             copies += [links.copy(("wc", dy, 0, dc), origin, block, block, at_core(dc)) for dc in cs]
         return copies
 
-    def w_y_service(origin):
+    def w_y_service(origin, turned=False):
         for dy in ys:
             links.arrive(("wy", dy), w_block(origin, back_y(dy), x, c), at_sp(s), at=origin)
-        for copy in w_y_copies(origin):
+        for copy in w_y_copies(origin, turned):
             copy.start()
+
+    def w_x_turn(origin):
+        for dx in xs:
+            block = w_block(origin, y, back_x(dx), c)
+            links.arrive(("wx", 0, dx), block, at_dp(d), at=origin)
+            w_over_core(origin, 0, dx, block, None)
+            for dy in ys:
+                links.send(("wxy", dx, dy), block, block, at_y(dy), at=origin)
+
+    def w_turned(origin):
+        for dx in xs:
+            for dy in ys:
+                block = w_block(origin, back_y(dy), back_x(dx), c)
+                links.arrive(("wxy", dx, dy), block, at_dp(d), at=origin)
+                w_over_core(origin, dy, dx, block, None)
 
     def w_x_arrive(origin, dyo):
         for dx in xs:
@@ -373,7 +416,7 @@
     for src, dst, _ in downs:
         dst[d] = src[...]
     for src, dst in ups:
-        dst[y, d] = src[...]
+        dst[zo, y, d] = src[...]
     own_out = pl.ds(pl.multiple_of((s * dps + d) * part_out, part_out), part_out)
     w_g[own_out, :] = w_out[...]
 
@@ -435,82 +478,110 @@
         for dy in ys:
             links.send(("kvy", dy), block, block, at_y(dy), ok, at=zz)
 
-    def launch(role, block):
-        for way in (1, -1):
-            if nz > 1:
-                along_z(role, way, z, block, block, (z + way >= 0) & (z + way < nz))
+    def up_arrive(role, a, k, dy, dx):
+        got = ups[a][1].at[up_slot(k, dy, dx, c)]
+        links.arrive(role, got, at_dp(d))
+        return got
 
     down_x(0)
-    if nz > 1:
-        w_z_relay(0)
     down_x(1)
     down_y(0)
+    for a in range(3):
+        for dy in ys:
+            got = up_arrive(("uy", a, 0, dy), a, 0, dy, 0)
+            up_over_x(a, 0, dy, got)
+            up_over_core(a, 0, dy, 0, got)
     for it in range(2, len(items)):
         down_x(it)
-    for a, (src, dst) in enumerate(ups):
-        for dx in xs:
-            links.send(("ux", a, 0, dx), src, dst.at[y, d], at_x(dx))
-        for dy in ys:
-            got = dst.at[back_y(dy), d]
-            links.arrive(("uy", a, dy), got, at_dp(d))
-            for dx in xs:
-                links.send(("ux", a, dy, dx), got, got, at_x(dx))
-            for dc in cs:
-                links.send(("uc", a, dy, 0, dc), got, got, at_core(dc))
+    def up_z(a):
+        for k in zs:
+            got = up_arrive(("uz", a, k), a, k, 0, 0)
+            up_over_y(a, k, got)
+            up_over_x(a, k, 0, got)
+            up_over_core(a, k, 0, 0, got)
+
     settle_down(0)
     kv_g[s, :rows, :] = rms_scale(down(wld_g), kv_lat_gain[...]).astype(jnp.bfloat16)
-    launch("kv", kv_g.at[s])
+    own_kv = kv_g.at[s]
+    along_z("kv", 1, z, own_kv, own_kv, z < nz - 1)
+    along_z("kv", -1, z, own_kv, own_kv, z > zb)
     kv_over_y(z)
     for it in range(1, len(items)):
         down_y(it)
 
-    def up_spread(a):
-        dst = ups[a][1]
+    def up_diagonal(a):
+        for k in zs:
+            for dy in ys:
+                got = up_arrive(("uy", a, k, dy), a, k, dy, 0)
+                up_over_x(a, k, dy, got)
+                up_over_core(a, k, dy, 0, got)
+
+    def up_spread(a, k):
         for dy in range(ny):
             for dx in xs:
-                got = dst.at[back_y(dy), back_x(dx) * cores + c]
-                links.arrive(("ux", a, dy, dx), got, at_dp(d))
-                for dc in cs:
-                    links.send(("uc", a, dy, dx, dc), got, got, at_core(dc))
+                up_over_core(a, k, dy, dx, up_arrive(("ux", a, k, dy, dx), a, k, dy, dx))
 
     def settle_up(a):
-        dst = ups[a][1]
-        for dy in range(ny):
-            for dx in range(nx):
-                for dc in cs:
-                    got = dst.at[back_y(dy), back_x(dx) * cores + back_core(dc)]
-                    links.arrive(("uc", a, dy, dx, dc), got, at_dp(d))
+        for k in range(nzs):
+            for dy in range(ny):
+                for dx in range(nx):
+                    for dc in cs:
+                        got = ups[a][1].at[up_slot(k, dy, dx, back_core(dc))]
+                        links.arrive(("uc", a, k, dy, dx, dc), got, at_dp(d))
 
     settle_down(1)
-    q_g[z] = rms_scale(down(wqd_g), q_lat_gain[...]).astype(jnp.bfloat16)
-
-    def z_relay(role, step, buffer, after=None, lazy=False):
+    q_g[zl] = rms_scale(down(wqd_g), q_lat_gain[...]).astype(jnp.bfloat16)
+
+    def kv_relay(step):
         for way in (1, -1):
             origin, ok, more = z_arrival(step, way)
-            block = buffer(origin)
-            links.arrive((role, way), block, at_sp(s), more if lazy else ok, at=origin)
-            along_z(role, way, origin, block, block, more)
-            if after is not None:
-                after(origin, ok)
-
-    def kv_block(zz):
-        return kv_g.at[zz * ny + y]
+            if way < 0:
+                base = origin - lax.rem(origin, group)
+                ok, more = ok & (z >= base), more & (z - 1 >= base)
+            block = kv_g.at[origin * ny + y]
+            links.arrive(("kv", way), block, at_sp(s), ok, at=origin)
+            along_z("kv", way, origin, block, block, more)
+            kv_over_y(origin, ok)
 
     for a in range(3):
-        up_spread(a)
+        up_z(a)
     if nz > 1:
-        z_relay("kv", 0, kv_block, kv_over_y)
+        kv_relay(0)
+    if nz > 1:
+        w_z_relay(0)
+    for a in range(3):
+        up_diagonal(a)
+    for step in range(1, nz - 2):
+        kv_relay(step)
+    for k in range(1, group):
+        links.send(("q", k), q_g.at[zl], q_g.at[zl], at_z(zb + lax.rem(zl + k, group)), at=zl)
     w_over_x(z, 0, w_out, None)
     w_over_core(z, 0, 0, w_out, None)
     if nz > 1:
         w_z_spread(0)
+    w_over_y(z, w_out, None)
+    for a in range(3):
+        up_spread(a, 0)
+    for k in zs:
+        for a in range(3):
+            up_spread(a, k)
     for a in range(3):
         settle_up(a)
-    shard_heads = heads // ny
+    for step in range(max(nz - 2, 1), nz - 1):
+        kv_relay(step)
+    for k in range(1, min(2, nz)):
+        w_y_near(k)
+    for step in range(1, nz - 2):
+        w_z_relay(step)
+        w_z_spread(step)
+    for k in range(2, nz - 1):
+        w_y_near(k)
+    shards = nzs * ny
+    shard_heads = heads // shards
     depth = wqu.shape[0]
-    for yy in range(ny):
+    for yy in range(shards):
         for k in range(dps):
-            up = wqu_g[yy, k].astype(jnp.float32)
+            up = wqu_g[yy // ny, yy % ny, k].astype(jnp.float32)
             width = wqu.shape[1] // shard_heads
             for h in range(shard_heads):
                 head = up[:, h * width : (h + 1) * width]
@@ -518,7 +589,7 @@
                 wide = both.shape[1]
                 first = (yy * shard_heads + h) * wide
                 wq_s[k * depth : (k + 1) * depth, first : first + wide] = both.astype(jnp.bfloat16)
-        wv = wvu_g[yy].reshape(dps * wvu.shape[0], wvu.shape[1])
+        wv = wvu_g[yy // ny, yy % ny].reshape(dps * wvu.shape[0], wvu.shape[1])
         wvt[yy * shard_heads * vd : (yy + 1) * shard_heads * vd, :] = jnp.transpose(
             wv.astype(jnp.float32)
         ).astype(jnp.bfloat16)
@@ -528,7 +599,7 @@
 
     def project_kv(block):
         tok = pl.ds(pl.multiple_of(block * rows, rows), rows)
-        wks = [wku_g[yy].reshape(dps * wku.shape[0], wku.shape[1]) for yy in range(ny)]
+        wks = [wku_g[yy // ny, yy % ny].reshape(dps * wku.shape[0], wku.shape[1]) for yy in range(shards)]
         shared = unpack_rope(kv_g[block, rows:, :], rope2)
         project_keys(block, rows, nope, kv_g[block, :rows, :], shared, wks, wvt, gk, table[tok, :] * gk2, k_s, v_s)
 
@@ -544,104 +615,120 @@
 
     def kv_columns(first, last):
         def one(i, _):
-            kv_column(near(i))
+            inside = zb + lax.rem(zl + i, group)
+            kv_column(jnp.where(i < group, inside, zb - 1 - (i - group)))
             return 0
 
         lax.fori_loop(first, last, one, 0)
 
-
-    def q_block(zz):
-        return q_g.at[zz]
-
-    for step in range(1, nz - 2):
-        z_relay("kv", step, kv_block, kv_over_y)
-    launch("q", q_g.at[z])
     kv_columns(0, 1)
-    for step in range(max(nz - 2, 1), nz - 1):
-        z_relay("kv", step, kv_block, kv_over_y)
-    for step in range(1, nz - 2):
-        w_z_relay(step, False)
-        w_z_spread(step)
-        z_relay("q", step - 1, q_block, lazy=True)
-    for step in range(1, nz - 2):
-        w_z_onward(step)
-    w_over_y(z, w_out, None)
-    for k in range(1, nz - 1):
-        w_y_near(k)
-    kv_columns(1, nz)
-    w_y_service(z)
-
-    def hand_over(zz):
-        return links.copy("a2a", zz, att_s.at[zz], heads_g.at[z], at_z(zz), land=z)
+    kv_columns(1, zb + group)
+    def hand_over(li):
+        return links.copy("a2a", li, att_s.at[li], heads_g.at[zl], at_z(zb + li), land=zl)
 
     def attend(i, _):
-        zz = near(i)
-        low = zz < z
-        last = jnp.where(low, z == nz - 1, z == 0)
-        for way, side in ((1, low), (-1, zz > z)):
-            links.arrive(("q", way), q_g.at[zz], at_sp(s), side & last, at=zz)
+        li = lax.rem(zl + 1 + i, group)
+        for k in range(1, group):
+            links.arrive(("q", k), q_g.at[li], at_sp(s), li == lax.rem(zl - k + group, group), at=li)
+        zz = zb + li
         qb = zz * ny + y
         tok = pl.ds(pl.multiple_of(qb * rows, rows), rows)
-        project_queries(rows, heads, nope, q_g[zz], wq_s, gq, table[tok, :] * gq2, q_s)
-        att_s[zz] = attend_block(zz, y, rows, chunk, heads, vd, scale, q_s, k_s, v_s, m_s, l_s, acc_s, scores)
-
-        @pl.when(i > 0)
+        project_queries(rows, heads, nope, q_g[li], wq_s, gq, table[tok, :] * gq2, q_s)
+        att_s[li] = attend_block(zz, y, rows, chunk, heads, vd, scale, q_s, k_s, v_s, m_s, l_s, work)
+
+        @pl.when(i < group - 1)
         def _():
-            hand_over(zz).start()
-        @pl.when((i > 0) & (i < nz - 2))
+            hand_over(li).start()
+
+        @pl.when(i == 0)
         def _():
-            w_y_service(near(i + 1))
+            for k in range(2, nz):
+                w_y_service(near(k), k < TURNED)
 
         return 0
 
-    lax.fori_loop(0, 1, attend, 0)
-    if nz > 1:
-        w_y_service(near(1))
-    for step in range(1, nz - 1):
-        z_relay("q", step, q_block, lazy=True)
     for step in range(max(nz - 2, 1), nz - 1):
         w_z_relay(step, False)
         w_z_spread(step)
     if nz > 2:
         w_y_near(nz - 1)
-    lax.fori_loop(1, max(nz - 1, 1), attend, 0)
-    if nz > 2:
-        w_y_service(near(nz - 1))
-    lax.fori_loop(max(nz - 1, 1), nz, attend, 0)
-    for k in range(nz):
-        for dy in range(ny):
-            w_x_arrive(lax.rem(z + k, nz), dy)
-    heads_g[z] = att_s[z]
-    for k in range(1, nz):
-        origin = lax.rem(z + k, nz)
-        links.copy("a2a", origin, att_s.at[origin], heads_g.at[z], at_z(origin), land=origin).wait_send()
-        links.copy("a2a", origin, heads_g.at[origin], heads_g.at[origin], at_z(origin), land=origin).wait_recv()
+
+    for k in range(min(TURNED, nz)):
+        w_x_turn(near(k))
+    w_y_service(z, TURNED > 0)
+    if nz > 1:
+        w_y_service(near(1), TURNED > 1)
+    lax.fori_loop(0, group, attend, 0)
+    heads_g[zl] = att_s[zl]
+    for k in range(1, group):
+        li = lax.rem(zl + k, group)
+        hand_over(li).wait_send()
+        links.copy("a2a", li, heads_g.at[li], heads_g.at[li], at_z(zb + li), land=li).wait_recv()
     width = heads * vd
+    band = width // nzs
     square = jnp.zeros((rows, 1), jnp.float32)
-    for k in range(nz):
+    for k in range(group):
         block = heads_g[k].astype(jnp.float32)
         square = square + jnp.sum(block * block, axis=-1, keepdims=True)
-    r = lax.rsqrt(square * (1.0 / (nz * width)) + EPS)
+    r = lax.rsqrt(square * (1.0 / (group * width)) + EPS)
+    for k in range(group):
+        for j in range(nzs):
+            cols = slice((j * group + k) * band, (j * group + k + 1) * band)
+            part = heads_g[k, :, j * band : (j + 1) * band].astype(jnp.float32)
+            normed[:, cols] = (part * r * out_gain[:, cols]).astype(jnp.bfloat16)
     for k in range(nz):
-        cols = slice(k * width, (k + 1) * width)
-        normed[:, cols] = (heads_g[k].astype(jnp.float32) * r * out_gain[:, cols]).astype(jnp.bfloat16)
-    for k in range(nz):
-        origin = lax.rem(z + k, nz)
-        for dy in range(ny):
+        if k >= TURNED:
+            w_x_arrive(near(k), 0)
+
+    def settle_w(dy):
+        for k in range(nz):
             for dx in range(nx):
                 for dc in cs:
-                    block = w_block(origin, back_y(dy), back_x(dx), back_core(dc))
-                    links.arrive(("wc", dy, dx, dc), block, at_dp(d), at=origin)
-    tile = 256 if out.shape[1] % 256 == 0 else out.shape[1]
-
-    def project_out(i, _):
+                    block = w_block(near(k), back_y(dy), back_x(dx), back_core(dc))
+                    links.arrive(("wc", dy, dx, dc), block, at_dp(d), at=near(k))
+
+    settle_w(0)
+    tile = rows * max(1, 512 // rows)
+    run = dps * part_out
+
+    def partial_out(yy, cols):
+        total = None
+        for zz in range(nz):
+            first = pl.multiple_of((zz * ny + yy) * run, run)
+            term = jnp.dot(normed[:, pl.ds(first, run)], w_g[pl.ds(first, run), cols], preferred_element_type=jnp.float32)
+            total = term if total is None else total + term
+        return total
+
+    def project_own(i, _):
         cols = pl.ds(pl.multiple_of(i * tile, tile), tile)
-        out[:, cols] = jnp.dot(normed[...], w_g[:, cols], preferred_element_type=jnp.float32).astype(out.dtype)
+        total = partial_out(y, cols)
+        for j in range(tile // rows):
+            at = pl.multiple_of(i * tile + j * rows, rows)
+            work[pl.ds(at, rows), :] = total[:, j * rows : (j + 1) * rows]
         return 0
 
-    lax.fori_loop(0, out.shape[1] // tile, project_out, 0)
+    lax.fori_loop(0, out.shape[1] // tile, project_own, 0)
     for k in range(nz):
-        for copy in w_y_copies(lax.rem(z + k, nz)):
+        if k < TURNED:
+            w_turned(near(k))
+            continue
+        for dy in ys:
+            w_x_arrive(near(k), dy)
+    for dy in ys:
+        settle_w(dy)
+
+    def project_rest(i, _):
+        cols = pl.ds(pl.multiple_of(i * tile, tile), tile)
+        at = pl.multiple_of(i * tile, tile)
+        total = jnp.concatenate([work[pl.ds(at + j * rows, rows), :] for j in range(tile // rows)], axis=1)
+        for dy in ys:
+            total = total + partial_out(back_y(dy), cols)
+        out[:, cols] = total.astype(out.dtype)
+        return 0
+
+    lax.fori_loop(0, out.shape[1] // tile, project_rest, 0)
+    for k in range(nz):
+        for copy in w_y_copies(near(k), k < TURNED):
             copy.wait_send()
     links.drain()
 
@@ -655,15 +742,17 @@
     nx = dps // cores
     ny = nx if seqs % nx == 0 else 1
     nz = seqs // ny
-    heads = HEADS // nz
+    group = 2 if nz % 2 == 0 else nz
+    heads = HEADS // group
+    shards = seqs // group
     own_rows = tokens.shape[1]
     length = own_rows * seqs
     rope = w_rope_key.shape[1]
-    nope = w_key_up.shape[1] * ny // heads
-    vd = w_value_up.shape[1] * ny // heads
+    nope = w_key_up.shape[1] * shards // heads
+    vd = w_value_up.shape[1] * shards // heads
     wide = nope + 2 * rope
     chunk = ny * own_rows
-    sems, sem_rows = sem_counts(nx, ny, nz, cores)
+    sems, sem_rows = sem_counts(nx, ny, nz, cores, group)
     b16 = jnp.bfloat16
 
     def gathered(w, *lead):
@@ -671,7 +760,7 @@
 
     result = pl.pallas_call(
         functools.partial(
-            layer_kernel, (nx, ny, nz, cores), chunk, heads, nope, vd, float(nope + rope) ** -0.5
+            layer_kernel, (nx, ny, nz, cores, group), chunk, heads, nope, vd, float(nope + rope) ** -0.5
         ),
         out_shape=jax.ShapeDtypeStruct((own_rows, w_out.shape[1]), b16),
         in_specs=[pl.BlockSpec(memory_space=pltpu.VMEM)] * 15,
@@ -679,28 +768,27 @@
         scratch_shapes=[
             pltpu.VMEM((own_rows, max(tokens.shape[2], w_out.shape[0] * seqs * dps)), b16),
             gathered(w_query_down), gathered(w_latent_down),
-            gathered(w_query_up, ny), gathered(w_key_up, ny), gathered(w_value_up, ny),
+            gathered(w_query_up, nz // group, ny), gathered(w_key_up, nz // group, ny), gathered(w_value_up, nz // group, ny),
             pltpu.VMEM((w_out.shape[0] * seqs * dps, w_out.shape[1]), b16),
             pltpu.VMEM((w_query_down.shape[1], heads * wide), b16),
             pltpu.VMEM((heads * vd, w_latent_down.shape[1]), b16),
             pltpu.VMEM((seqs, own_rows + own_rows * rope // w_latent_down.shape[1], w_latent_down.shape[1]), b16),
-            pltpu.VMEM((nz, own_rows, w_query_down.shape[1]), b16),
+            pltpu.VMEM((group, own_rows, w_query_down.shape[1]), b16),
             pltpu.VMEM((heads, own_rows, wide), b16),
             pltpu.VMEM((heads, length, wide), b16),
             pltpu.VMEM((heads * vd, length), b16),
             pltpu.VMEM((heads, 1, own_rows), jnp.float32),
             pltpu.VMEM((heads, 1, own_rows), jnp.float32),
-            pltpu.VMEM((heads, vd, own_rows), jnp.float32),
-            pltpu.VMEM((heads, chunk, own_rows), jnp.float32),
-            pltpu.VMEM((nz, own_rows, heads * vd), b16),
-            pltpu.VMEM((nz, own_rows, heads * vd), b16),
+            pltpu.VMEM((max(heads * vd + 2 * chunk, w_out.shape[1]), own_rows), jnp.float32),
+            pltpu.VMEM((group, own_rows, heads * vd), b16),
+            pltpu.VMEM((group, own_rows, heads * vd), b16),
             pltpu.SemaphoreType.DMA((sems,)),
             pltpu.SemaphoreType.DMA((sems,)),
             pltpu.SemaphoreType.DMA((sem_rows, nz)),
             pltpu.SemaphoreType.DMA((sem_rows, nz)),
         ],
         compiler_params=pltpu.CompilerParams(
-            vmem_limit_bytes=56 * 1024 * 1024, collective_id=0, has_side_effects=True
+            vmem_limit_bytes=62 * 1024 * 1024, collective_id=0, has_side_effects=True
         ),
         cost_estimate=pl.CostEstimate(flops=60 * 10**9, bytes_accessed=10**8, transcendentals=5 * 10**6),
     )(

time: 91.9 us -> 84.3 us (0.917)
  the two profiles are of different devices: /device:TPU:0 before, /device:TPU:25 now
where the time goes in v3:
time: 84.3 us; the launch traced here: 84.2 us
  Pallas kernels  81.9 us (97%)
  local copies, waits for them, and re-layouts  2.3 us (3%)
    pallas_call x1, Pallas kernels, per_device(): pl.pallas_call(functools.partial(layer_kernel, (nx, ny, nz, cores, group)...  81.9 us
    unnamed x1, local copies, waits for them, and re-layouts  2.3 us

profile of v3, /device:TPU:25, one launch (start us, length us, event | category | flops | bytes accessed | tf_op | source)
XLA Modules:
  0.0 84.2 jit_solution(11973518932050933672)
XLA Ops:
  0.0 81.9 %shard_map.145 = bf16[256,2048]{1,0:T(8,128)(2,1)} custom-call(bf16[256,2048]{1,0:T(8,128)(2,1)} %bitcast.10, f32[1,2048]{1,0:T(1,128)} %bitcast.12, bf16[512,512]{1,0:T(8,128)(2,1)} %wqd.1, bf16[512,256]{1,0:T(8,128)(2,1)} %wld.1, bf16[64,2048]{1,0:T(8,128)(2,1)} %bitcast.11, f32[1,512]{1,0:T(1,128)} %bitcast.14, f32[1,256]{1,0:T(1,128)} %bitcast.15, ...), custom_call_target="tpu_custom_call" | custom-call | flops 60000002048 | bytes 100000000 | tf_op jit(solution)/shard_map/pallas_call | solution.py:761
  81.9 2.3 %copy.17 = bf16[1,256,2048]{2,1,0:T(8,128)(2,1)} copy(bf16[1,256,2048]{2,1,0:T(8,128)(2,1)} %bitcast.9) | data formatting | bytes 2097152

commit v4 on v3

--- a/solution.py
+++ b/solution.py
@@ -144,7 +144,7 @@
         )
 
 
-def attend_block(i, y, rows, chunk, heads, vd, scale, q_s, k_s, v_s, m_s, l_s, work):
+def attend_block(i, y, rows, chunk, heads, vd, scale, q_s, k_s, v_s, m_s, l_s, work, between):
     m_s[...] = jnp.full(m_s.shape, NEG_BIG, jnp.float32)
     l_s[...] = jnp.zeros(l_s.shape, jnp.float32)
     work[0 : heads * vd, :] = jnp.zeros((heads * vd, rows), jnp.float32)
@@ -157,6 +157,7 @@
         return 0
 
     lax.fori_loop(0, i, step, 0)
+    between()
     item(i, True)
     return jnp.concatenate([jnp.transpose(work[h * vd : (h + 1) * vd, :] / l_s[h]) for h in range(heads)], axis=1).astype(jnp.bfloat16)
 
@@ -205,7 +206,7 @@
 
 
 DOWN_CUTS = (1, 2)
-TURNED = 2
+TURNED = 1
 
 
 def sem_counts(nx, ny, nz, cores, group):
@@ -220,14 +221,16 @@
 
 def layer_kernel(
     dims, chunk, heads, nope, vd, scale,
-    tokens, in_gain, wqd, wld, wrope, q_lat_gain, kv_lat_gain, wqu, wku, wvu, q_gain, k_gain, table, out_gain, w_out,
+    tokens_in, in_gain_in, wqd_in, wld_in, wrope_in, q_lat_gain_in, kv_lat_gain_in, wqu_in, wku_in, wvu_in,
+    q_gain_in, k_gain_in, table_in, out_gain_in, w_out_in,
     out,
+    in_gain, wrope, q_lat_gain, kv_lat_gain, q_gain, k_gain, table, out_gain,
     normed, wqd_g, wld_g, wqu_g, wku_g, wvu_g, w_g, wq_s, wvt, kv_g, q_g, q_s, k_s, v_s, m_s, l_s, work, att_s, heads_g,
-    send_sems, recv_sems, send_rows, recv_rows,
+    send_sems, recv_sems, send_rows, recv_rows, load_sems,
 ):
     nx, ny, nz, cores, group = dims
     seqs, dps = ny * nz, nx * cores
-    rows = tokens.shape[0]
+    rows = tokens_in.shape[0]
     s, d = lax.axis_index("sp"), lax.axis_index("dp")
     y, z = lax.rem(s, ny), lax.div(s, ny)
     c, x = lax.rem(d, cores), lax.div(d, cores)
@@ -235,6 +238,24 @@
     zb, nzs = z - zl, nz // group
     links = Links(send_sems, recv_sems, send_rows, recv_rows)
 
+    part_out = w_out_in.shape[0]
+
+    def w_block(zz, yy, xx, cc):
+        first = ((zz * ny + yy) * dps + xx * cores + cc) * part_out
+        return w_g.at[pl.ds(pl.multiple_of(first, part_out), part_out)]
+
+    wqd, wld, w_out = wqd_g.at[d], wld_g.at[d], w_block(z, y, x, c)
+    wqu, wku, wvu = wqu_g.at[zo, y, d], wku_g.at[zo, y, d], wvu_g.at[zo, y, d]
+    pairs = (
+        (wld_in, wld), (wqd_in, wqd), (wqu_in, wqu), (wku_in, wku), (wvu_in, wvu), (w_out_in, w_out),
+        (tokens_in, normed), (in_gain_in, in_gain), (wrope_in, wrope), (q_lat_gain_in, q_lat_gain),
+        (kv_lat_gain_in, kv_lat_gain), (q_gain_in, q_gain), (k_gain_in, k_gain), (table_in, table),
+        (out_gain_in, out_gain),
+    )
+    loads = [pltpu.make_async_copy(src, dst, load_sems.at[n]) for n, (src, dst) in enumerate(pairs)]
+    for load in loads:
+        load.start()
+
     def at_sp(target):
         return {"sp": target, "dp": d}
 
@@ -275,6 +296,9 @@
     for peer in peers:
         pl.semaphore_signal(barrier, inc=1, device_id=peer, device_id_type=MESH)
     pl.semaphore_wait(barrier, len(peers))
+
+    for load in loads[:6]:
+        load.wait()
 
     xs, ys, cs, zs = range(1, nx), range(1, ny), range(1, cores), range(1, nzs)
 
@@ -319,12 +343,6 @@
         up_over_y(a, 0, src)
         up_over_x(a, 0, 0, src)
         up_over_core(a, 0, 0, 0, src)
-
-    part_out = w_out.shape[0]
-
-    def w_block(zz, yy, xx, cc):
-        first = ((zz * ny + yy) * dps + xx * cores + cc) * part_out
-        return w_g.at[pl.ds(pl.multiple_of(first, part_out), part_out)]
 
     def along_z(role, way, origin, src, dst, ok):
         links.send((role, way), src, dst, at_z(jnp.clip(z + way, 0, nz - 1)), ok, at=origin)
@@ -413,17 +431,13 @@
         if nz > 1:
             along_z("wz", way, z, w_out, own_block, (z + way >= 0) & (z + way < nz))
 
-    for src, dst, _ in downs:
-        dst[d] = src[...]
-    for src, dst in ups:
-        dst[zo, y, d] = src[...]
-    own_out = pl.ds(pl.multiple_of((s * dps + d) * part_out, part_out), part_out)
-    w_g[own_out, :] = w_out[...]
+    for load in loads[6:]:
+        load.wait()
 
     def norm(i, _):
         step = rows // 4
         band = pl.ds(pl.multiple_of(i * step, step), step)
-        normed[band, :] = rms_scale(tokens[band, :].astype(jnp.float32), in_gain[...]).astype(jnp.bfloat16)
+        normed[band, :] = rms_scale(normed[band, :].astype(jnp.float32), in_gain[...]).astype(jnp.bfloat16)
         return 0
 
     lax.fori_loop(0, 4, norm, 0)
@@ -567,15 +581,9 @@
             up_spread(a, k)
     for a in range(3):
         settle_up(a)
-    for step in range(max(nz - 2, 1), nz - 1):
-        kv_relay(step)
-    for k in range(1, min(2, nz)):
-        w_y_near(k)
     for step in range(1, nz - 2):
         w_z_relay(step)
         w_z_spread(step)
-    for k in range(2, nz - 1):
-        w_y_near(k)
     shards = nzs * ny
     shard_heads = heads // shards
     depth = wqu.shape[0]
@@ -622,11 +630,41 @@
         lax.fori_loop(first, last, one, 0)
 
     kv_columns(0, 1)
+    for step in range(max(nz - 2, 1), nz - 1):
+        kv_relay(step)
+    for k in range(1, min(2, nz)):
+        w_y_near(k)
+    for k in range(2, nz - 1):
+        w_y_near(k)
     kv_columns(1, zb + group)
     def hand_over(li):
         return links.copy("a2a", li, att_s.at[li], heads_g.at[zl], at_z(zb + li), land=zl)
 
-    def attend(i, _):
+    def far_w():
+        for step in range(max(nz - 2, 1), nz - 1):
+            w_z_relay(step, False)
+            w_z_spread(step)
+        if nz > 2:
+            w_y_near(nz - 1)
+
+    def turn_w(k):
+        if k < nz:
+            if k < TURNED:
+                w_x_turn(near(k))
+            w_y_service(near(k), k < TURNED)
+
+    def early():
+        far_w()
+        turn_w(1)
+
+    def late():
+        turn_w(2)
+
+    def rest():
+        for k in range(3, nz):
+            turn_w(k)
+
+    def attend(i, between):
         li = lax.rem(zl + 1 + i, group)
         for k in range(1, group):
             links.arrive(("q", k), q_g.at[li], at_sp(s), li == lax.rem(zl - k + group, group), at=li)
@@ -634,31 +672,18 @@
         qb = zz * ny + y
         tok = pl.ds(pl.multiple_of(qb * rows, rows), rows)
         project_queries(rows, heads, nope, q_g[li], wq_s, gq, table[tok, :] * gq2, q_s)
-        att_s[li] = attend_block(zz, y, rows, chunk, heads, vd, scale, q_s, k_s, v_s, m_s, l_s, work)
-
-        @pl.when(i < group - 1)
-        def _():
+        att_s[li] = attend_block(
+            zz, y, rows, chunk, heads, vd, scale, q_s, k_s, v_s, m_s, l_s, work, between
+        )
+        if i < group - 1:
             hand_over(li).start()
 
-        @pl.when(i == 0)
-        def _():
-            for k in range(2, nz):
-                w_y_service(near(k), k < TURNED)
-
-        return 0
-
-    for step in range(max(nz - 2, 1), nz - 1):
-        w_z_relay(step, False)
-        w_z_spread(step)
-    if nz > 2:
-        w_y_near(nz - 1)
-
-    for k in range(min(TURNED, nz)):
-        w_x_turn(near(k))
-    w_y_service(z, TURNED > 0)
-    if nz > 1:
-        w_y_service(near(1), TURNED > 1)
-    lax.fori_loop(0, group, attend, 0)
+    turn_w(0)
+    for i in range(group):
+        attend(i, early if i == 0 else late if i == 1 else lambda: None)
+    if group < 2:
+        late()
+    rest()
     heads_g[zl] = att_s[zl]
     for k in range(1, group):
         li = lax.rem(zl + k, group)
@@ -680,53 +705,53 @@
         if k >= TURNED:
             w_x_arrive(near(k), 0)
 
-    def settle_w(dy):
-        for k in range(nz):
-            for dx in range(nx):
-                for dc in cs:
-                    block = w_block(near(k), back_y(dy), back_x(dx), back_core(dc))
-                    links.arrive(("wc", dy, dx, dc), block, at_dp(d), at=near(k))
-
-    settle_w(0)
+    def settle_w(origin, dy):
+        for dx in range(nx):
+            for dc in cs:
+                block = w_block(origin, back_y(dy), back_x(dx), back_core(dc))
+                links.arrive(("wc", dy, dx, dc), block, at_dp(d), at=origin)
+
+    for k in range(nz):
+        settle_w(near(k), 0)
     tile = rows * max(1, 512 // rows)
     run = dps * part_out
 
-    def partial_out(yy, cols):
-        total = None
-        for zz in range(nz):
-            first = pl.multiple_of((zz * ny + yy) * run, run)
-            term = jnp.dot(normed[:, pl.ds(first, run)], w_g[pl.ds(first, run), cols], preferred_element_type=jnp.float32)
-            total = term if total is None else total + term
-        return total
-
-    def project_own(i, _):
-        cols = pl.ds(pl.multiple_of(i * tile, tile), tile)
-        total = partial_out(y, cols)
-        for j in range(tile // rows):
-            at = pl.multiple_of(i * tile + j * rows, rows)
-            work[pl.ds(at, rows), :] = total[:, j * rows : (j + 1) * rows]
-        return 0
-
-    lax.fori_loop(0, out.shape[1] // tile, project_own, 0)
-    for k in range(nz):
+    def add_out(blocks, first, last):
+        def one(i, _):
+            at = pl.multiple_of(i * tile, tile)
+            cols = pl.ds(at, tile)
+            held = [work.at[pl.ds(pl.multiple_of(at + j * rows, rows), rows)] for j in range(tile // rows)]
+            total = None if first else jnp.concatenate([h[...] for h in held], axis=1)
+            for zz, yy in blocks:
+                at_rows = pl.ds(pl.multiple_of((zz * ny + yy) * run, run), run)
+                term = jnp.dot(normed[:, at_rows], w_g[at_rows, cols], preferred_element_type=jnp.float32)
+                total = term if total is None else total + term
+            if last:
+                out[:, cols] = total.astype(out.dtype)
+            else:
+                for j in range(tile // rows):
+                    held[j][...] = total[:, j * rows : (j + 1) * rows]
+            return 0
+
+        lax.fori_loop(0, out.shape[1] // tile, one, 0)
+
+    def finish_w(k):
         if k < TURNED:
             w_turned(near(k))
-            continue
-        for dy in ys:
-            w_x_arrive(near(k), dy)
-    for dy in ys:
-        settle_w(dy)
-
-    def project_rest(i, _):
-        cols = pl.ds(pl.multiple_of(i * tile, tile), tile)
-        at = pl.multiple_of(i * tile, tile)
-        total = jnp.concatenate([work[pl.ds(at + j * rows, rows), :] for j in range(tile // rows)], axis=1)
-        for dy in ys:
-            total = total + partial_out(back_y(dy), cols)
-        out[:, cols] = total.astype(out.dtype)
-        return 0
-
-    lax.fori_loop(0, out.shape[1] // tile, project_rest, 0)
+        else:
+            for dy in ys:
+                w_x_arrive(near(k), dy)
+
+    add_out([(near(k), y) for k in range(nz)], True, ny == 1)
+    others = [[(near(k), back_y(dy)) for dy in ys] for k in range(nz)]
+    phases = ([k for k in range(nz - 1)], [nz - 1]) if nz > 1 else ([0],)
+    for phase in phases if ny > 1 else ():
+        for k in phase:
+            finish_w(k)
+        for k in phase:
+            for dy in ys:
+                settle_w(near(k), dy)
+        add_out(sum([others[k] for k in phase], []), False, phase is phases[-1])
     for k in range(nz):
         for copy in w_y_copies(near(k), k < TURNED):
             copy.wait_send()
@@ -762,11 +787,19 @@
         functools.partial(
             layer_kernel, (nx, ny, nz, cores, group), chunk, heads, nope, vd, float(nope + rope) ** -0.5
         ),
-        out_shape=jax.ShapeDtypeStruct((own_rows, w_out.shape[1]), b16),
-        in_specs=[pl.BlockSpec(memory_space=pltpu.VMEM)] * 15,
+        out_shape=pltpu.VMEM((own_rows, w_out.shape[1]), b16),
+        in_specs=[pl.BlockSpec(memory_space=pltpu.HBM)] * 15,
         out_specs=pl.BlockSpec(memory_space=pltpu.VMEM),
         scratch_shapes=[
-            pltpu.VMEM((own_rows, max(tokens.shape[2], w_out.shape[0] * seqs * dps)), b16),
+            pltpu.VMEM((1, tokens.shape[2]), jnp.float32),
+            pltpu.VMEM((rope, tokens.shape[2]), b16),
+            pltpu.VMEM((1, w_query_down.shape[1]), jnp.float32),
+            pltpu.VMEM((1, w_latent_down.shape[1]), jnp.float32),
+            pltpu.VMEM((1, nope + rope), jnp.float32),
+            pltpu.VMEM((1, nope + rope), jnp.float32),
+            pltpu.VMEM((length, 2 * rope), jnp.float32),
+            pltpu.VMEM((1, out_gain.shape[0]), jnp.float32),
+            pltpu.VMEM((own_rows, tokens.shape[2]), b16),
             gathered(w_query_down), gathered(w_latent_down),
             gathered(w_query_up, nz // group, ny), gathered(w_key_up, nz // group, ny), gathered(w_value_up, nz // group, ny),
             pltpu.VMEM((w_out.shape[0] * seqs * dps, w_out.shape[1]), b16),
@@ -786,9 +819,10 @@
             pltpu.SemaphoreType.DMA((sems,)),
             pltpu.SemaphoreType.DMA((sem_rows, nz)),
             pltpu.SemaphoreType.DMA((sem_rows, nz)),
+            pltpu.SemaphoreType.DMA((15,)),
         ],
         compiler_params=pltpu.CompilerParams(
-            vmem_limit_bytes=62 * 1024 * 1024, collective_id=0, has_side_effects=True
+            vmem_limit_bytes=min(62, 56 * length // 2048) * 1024 * 1024, collective_id=0, has_side_effects=True
         ),
         cost_estimate=pl.CostEstimate(flops=60 * 10**9, bytes_accessed=10**8, transcendentals=5 * 10**6),
     )(

time: 84.3 us -> 77.2 us (0.916)
  Pallas kernels: 81.9 us -> 76 us
  local copies, waits for them, and re-layouts: 2.3 us -> 0.97 us
    pallas_call x1, Pallas kernels: 81.9 us -> 76 us  [per_device(): pl.pallas_call(functools.partial(layer_kernel, (nx, ny, nz, cores, group)...]
    unnamed x1, local copies, waits for them, and re-layouts: 2.3 us -> 0.97 us
where the time goes in v4:
time: 77.2 us; the launch traced here: 77 us
  Pallas kernels  76 us (98%)
  local copies, waits for them, and re-layouts  0.97 us (1%)
    pallas_call x1, Pallas kernels, per_device(): pl.pallas_call(functools.partial(layer_kernel, (nx, ny, nz, cores, group)...  76 us

profile of v4, /device:TPU:25, one launch (start us, length us, event | category | flops | bytes accessed | tf_op | source)
XLA Modules:
  0.0 77.0 jit_solution(8310471136860574905)
XLA Ops:
  0.0 76.0 %shard_map.145 = bf16[256,2048]{1,0:T(8,128)(2,1)S(1)} custom-call(bf16[256,2048]{1,0:T(8,128)(2,1)} %bitcast.10, f32[1,2048]{1,0:T(1,128)} %bitcast.12, bf16[512,512]{1,0:T(8,128)(2,1)} %wqd_in.1, bf16[512,256]{1,0:T(8,128)(2,1)} %wld_in.1, bf16[64,2048]{1,0:T(8,128)(2,1)} %bitcast.11, f32[1,512]{1,0:T(1,128)} %bitcast.14, f32[1,256]{1,0:T(1,128)} %bitcast.15, ...), custom_call_target="tpu_custom_call" | custom-call | flops 60000002048 | bytes 100000000 | tf_op jit(solution)/shard_map/pallas_call | solution.py:786
  76.0 1.0 %copy.17 = bf16[1,256,2048]{2,1,0:T(8,128)(2,1)} copy(bf16[1,256,2048]{2,1,0:T(8,128)(2,1)S(1)} %bitcast.9) | data formatting | bytes 2097152
